TPU v7x, 512 devices: a whole 4x8x8 slice. The times are simulated.
512 devices in a mesh: sp: 64 (over z, y), tp: 8 (over x, core).
Axes of the slice: x: 4, y: 8, z: 8, core: 2. Of those that a mesh axis runs over, the one named last changes fastest.
Arguments:
- tokens: bfloat16 [24576, 2048], P('sp', 'tp'), may hold values from -6 to 6
- input_gain: float32 [2048], replicated, may hold values from 0.1 to 1.9
- query_weight: bfloat16 [2048, 1024], P(None, 'tp'), may hold values from -0.5 to 0.5
- query_rot_weight: bfloat16 [2048, 512], P(None, 'tp'), may hold values from -0.125 to 0.125
- kv_down: bfloat16 [2048, 256], replicated, may hold values from -0.5 to 0.5
- rot_down: bfloat16 [2048, 32], replicated, may hold values from -0.125 to 0.125
- kv_gain: float32 [256], replicated, may hold values from 0.1 to 1.9
- key_up: bfloat16 [256, 1024], P(None, 'tp'), may hold values from -0.5 to 0.5
- value_up: bfloat16 [256, 1024], P(None, 'tp'), may hold values from -4 to 4
- conv_value_weight: bfloat16 [2048, 1024], P(None, 'tp'), may hold values from -0.125 to 0.125
- conv_gate_weight: bfloat16 [2048, 1024], P(None, 'tp'), may hold values from -0.125 to 0.125
- conv_taps: float32 [31, 1024], P(None, 'tp'), may hold values from -8 to 8
- conv_ln_gain: float32 [1024], P('tp'), may hold values from 0.1 to 1.9
- conv_ln_bias: float32 [1024], P('tp'), may hold values from -3 to 3
- att_out_gain: float32 [1024], P('tp'), may hold values from 0.1 to 1.9
- conv_out_gain: float32 [1024], P('tp'), may hold values from 0.1 to 1.9
- att_out_weight: bfloat16 [1024, 2048], P('tp'), may hold values from -0.125 to 0.125
- conv_out_weight: bfloat16 [1024, 2048], P('tp'), may hold values from -0.125 to 0.125
Outputs:
- mixed: bfloat16 [24576, 2048], P('sp', 'tp')
All inputs are finite; a program needn't handle non-finite values.
Results may differ from a plain program's by a relative error of at most 0.017.
Values may be sent and summed in bfloat16 or wider, within the bound.
A program may use at most 128 MiB of HBM per device.

v0:
```python
import math

import jax
import jax.numpy as jnp
from jax import lax
from jax.sharding import PartitionSpec as P

D_MODEL = 2048
NOPE_DIM = 64
ROT_DIM = 32
VALUE_DIM = 64
CONV_CH = 1024
KERNEL = 31
ATT_WIDTH = 1024


norm_eps = 1e-06
far_below = -1e30
rope_base = 10000.0


def copy_for_each(x, axis):
    peers = lax.axis_size(axis)
    return lax.all_to_all(jnp.broadcast_to(x[None], (peers, *x.shape)), axis, 0, 0, tiled=True)


def in_order(pieces, dim):
    pieces = jnp.moveaxis(pieces, 0, dim)
    shape = pieces.shape
    return pieces.reshape(*shape[:dim], shape[dim] * shape[dim + 1], *shape[dim + 2 :])


def gathered_copies(x, axis, dim):
    pieces = copy_for_each(x, axis)
    return in_order(pieces, dim)


def sent_together(arrays, axis, dim, along):
    both = jnp.concatenate(arrays, axis=along)
    result, at, gathered = (lax.all_gather(both, axis, axis=dim, tiled=True), 0, [])
    for a in arrays:
        gathered.append(lax.slice_in_dim(result, at, at + a.shape[along], axis=along))
        at += a.shape[along]
    return tuple(gathered)


def shifted(block, axis, distance):
    devices = range(lax.axis_size(axis))
    route = [(i - distance, i) for i in devices if i - distance in devices]
    return lax.ppermute(block, axis, route)


def of_everyone(x, axis):
    everything = copy_for_each(x, axis)
    return jnp.sum(everything, axis=0)


def in_one(arrays, axis):
    line, at, gathered = (jnp.concatenate([a.reshape(-1) for a in arrays]), 0, [])
    so_far = of_everyone(line, axis)
    for a in arrays:
        gathered.append(so_far[at : at + a.size].reshape(a.shape))
        at += a.size
    return tuple(gathered)


def cut_along(x, dim, peers):
    shape = x.shape
    pieces = x.reshape(*shape[:dim], peers, shape[dim] // peers, *shape[dim + 1 :])
    return jnp.moveaxis(pieces, dim, 0)


def summed_on_arrival(x, axis, dim):
    pieces = cut_along(x, dim, lax.axis_size(axis))
    arrived = lax.all_to_all(pieces, axis, split_axis=0, concat_axis=0, tiled=True)
    return arrived.astype(jnp.float32).sum(axis=0)


def rotary_tables(positions, half_dim):
    frequency = rope_base ** (-jnp.arange(half_dim, dtype=jnp.float32) / half_dim)
    angles = positions.astype(jnp.float32)[:, None] * frequency[None, :]
    return (jnp.cos(angles), jnp.sin(angles))


def rotate_half(values, cos_table, sine_table):
    half_dim = cos_table.shape[-1]
    front_half = values[..., :half_dim]
    back_half = values[..., half_dim:]
    return jnp.concatenate(
        [
            front_half * cos_table - back_half * sine_table,
            back_half * cos_table + front_half * sine_table,
        ],
        axis=-1,
    )


def shards(
    tokens,
    input_gain,
    query_weight,
    query_rot_weight,
    kv_down,
    rot_down,
    kv_gain,
    key_up,
    value_up,
    conv_value_weight,
    conv_gate_weight,
    conv_taps,
    conv_ln_gain,
    conv_ln_bias,
    att_out_gain,
    conv_out_gain,
    att_out_weight,
    conv_out_weight,
):
    tok_rows = tokens.shape[0]
    heads_here = key_up.shape[1] // NOPE_DIM
    chan_here = conv_taps.shape[1]
    weight_list = (
        query_weight,
        query_rot_weight,
        kv_down,
        rot_down,
        conv_value_weight,
        conv_gate_weight,
    )
    wide_part = gathered_copies(tokens, "tp", 1).astype(jnp.float32)
    scaled = (wide_part * input_gain[None, :]).astype(jnp.bfloat16)

    def add_product(weight):
        return jnp.dot(scaled, weight, preferred_element_type=jnp.float32)

    summed = tuple((add_product(weight) for weight in weight_list))
    q_acc, qrot_acc, latent_raw, rot_acc, value_acc, gate_acc, square_sum = summed + (
        jnp.sum(wide_part * wide_part, axis=1),
    )
    row_scale = lax.rsqrt(square_sum / D_MODEL + norm_eps)[:, None]
    positions = lax.axis_index("sp") * tok_rows + jnp.arange(tok_rows, dtype=jnp.int32)
    cos_table, sine_table = rotary_tables(positions, ROT_DIM // 2)
    queries = (q_acc * row_scale).astype(jnp.bfloat16).reshape(tok_rows, heads_here, NOPE_DIM)
    query_rot = rotate_half(
        (qrot_acc * row_scale).reshape(tok_rows, heads_here, ROT_DIM),
        cos_table[:, None, :],
        sine_table[:, None, :],
    ).astype(jnp.bfloat16)
    latent = (
        latent_raw
        * lax.rsqrt(jnp.mean(latent_raw * latent_raw, axis=1, keepdims=True) + norm_eps)
        * kv_gain[None, :]
    ).astype(jnp.bfloat16)
    key_rot = rotate_half(rot_acc * row_scale, cos_table, sine_table).astype(jnp.bfloat16)
    gated_input = (value_acc * row_scale * jax.nn.sigmoid(gate_acc * row_scale)).astype(
        jnp.bfloat16
    )
    query_end = (lax.axis_index("sp") + 1) * tok_rows
    inv_scale = 1.0 / math.sqrt(NOPE_DIM + ROT_DIM)

    def attend(carried, key_block, rot_block, value_block, key_offset):
        run_max, run_sum, run_acc = carried
        block_len = key_block.shape[0]
        scores = (
            jnp.einsum("qhd,khd->hqk", queries, key_block, preferred_element_type=jnp.float32)
            + jnp.einsum("qhd,kd->hqk", query_rot, rot_block, preferred_element_type=jnp.float32)
        ) * inv_scale
        key_pos = key_offset + jnp.arange(block_len, dtype=jnp.int32)
        visible = (key_pos[None, :] <= positions[:, None])[None]
        new_max = jnp.maximum(run_max, jnp.max(jnp.where(visible, scores, far_below), axis=2))
        exp_scores = jnp.where(visible, jnp.exp(scores - new_max[:, :, None]), 0.0)
        shrink = jnp.exp(run_max - new_max)
        run_sum = run_sum * shrink + jnp.sum(exp_scores, axis=2)
        run_acc = run_acc * shrink.T[:, :, None] + jnp.einsum(
            "hqk,khd->qhd",
            exp_scores.astype(jnp.bfloat16),
            value_block,
            preferred_element_type=jnp.float32,
        )
        return (new_max, run_sum, run_acc)

    def reshape_heads(sliced):
        key_rows, value_rows, rot_block = sliced
        return (
            key_rows.reshape(-1, heads_here, NOPE_DIM),
            value_rows.reshape(-1, heads_here, VALUE_DIM),
            rot_block,
        )

    def square_rows(matrix):
        wide_rows = matrix.astype(jnp.float32)
        return jnp.sum(wide_rows * wide_rows, axis=1)

    rim_rows = shifted(gated_input[tok_rows - (KERNEL - 1) :], "sp", 1)
    padded = jnp.concatenate([rim_rows, gated_input], axis=0)
    conv_out = jnp.zeros((tok_rows, chan_here), jnp.float32)
    for tap_idx in range(KERNEL):
        conv_out = conv_out + conv_taps[tap_idx][None, :] * padded[
            tap_idx : tap_idx + tok_rows
        ].astype(jnp.float32)
    moment_one, moment_two = in_one(
        (jnp.sum(conv_out, axis=1), jnp.sum(conv_out * conv_out, axis=1)), "tp"
    )
    mean_val = moment_one / CONV_CH
    spread = moment_two / CONV_CH - mean_val * mean_val
    normed = (conv_out - mean_val[:, None]) * lax.rsqrt(spread + norm_eps)[:, None]
    swished = jax.nn.silu(normed * conv_ln_gain[None, :] + conv_ln_bias[None, :])
    start_state = (
        jnp.full((heads_here, tok_rows), far_below, jnp.float32),
        jnp.zeros((heads_here, tok_rows), jnp.float32),
        jnp.zeros((tok_rows, heads_here, VALUE_DIM), jnp.float32),
    )
    own_keys = jnp.dot(latent, key_up, preferred_element_type=jnp.float32).astype(jnp.bfloat16)
    own_values = jnp.dot(latent, value_up, preferred_element_type=jnp.float32).astype(jnp.bfloat16)
    pieces = sent_together((own_keys, own_values, key_rot), "sp", 0, 1)
    piece_rows = pieces[0].shape[0]
    step_len = math.gcd(piece_rows, 512)

    def visit_block(running, block_idx):
        start_row = block_idx * step_len
        sliced = tuple(
            (lax.dynamic_slice_in_dim(member, start_row, step_len, 0) for member in pieces)
        )

        def compute(current):
            key_block, value_block, rot_block = reshape_heads(sliced)
            return attend(current, key_block, rot_block, value_block, start_row)

        return (lax.cond(start_row < query_end, compute, lambda current: current, running), None)

    final_state = lax.scan(
        visit_block, start_state, jnp.arange(piece_rows // step_len, dtype=jnp.int32)
    )[0]
    run_max, run_sum, run_acc = final_state
    attended = (
        (run_acc / run_sum.T[:, :, None])
        .astype(jnp.bfloat16)
        .reshape(tok_rows, heads_here * VALUE_DIM)
    )
    att_sq, conv_sq = in_one((square_rows(attended), square_rows(swished)), "tp")
    att_mixed = (
        attended.astype(jnp.float32)
        * lax.rsqrt(att_sq / ATT_WIDTH + norm_eps)[:, None]
        * att_out_gain[None, :]
    ).astype(jnp.bfloat16)
    conv_mixed = (
        swished * lax.rsqrt(conv_sq / CONV_CH + norm_eps)[:, None] * conv_out_gain[None, :]
    ).astype(jnp.bfloat16)
    contract = (((0,), (1,)), ((), ()))
    feature_rows = summed_on_arrival(
        (
            lax.dot_general(att_out_weight, att_mixed, contract, preferred_element_type=jnp.float32)
            + lax.dot_general(
                conv_out_weight, conv_mixed, contract, preferred_element_type=jnp.float32
            )
        ).astype(jnp.bfloat16),
        "tp",
        0,
    )
    return feature_rows.T.astype(jnp.bfloat16)


def solution(mesh):
    return jax.shard_map(
        shards,
        mesh=mesh,
        in_specs=(
            P("sp", "tp"),
            P(),
            P(None, "tp"),
            P(None, "tp"),
            P(),
            P(),
            P(),
            P(None, "tp"),
            P(None, "tp"),
            P(None, "tp"),
            P(None, "tp"),
            P(None, "tp"),
            P("tp"),
            P("tp"),
            P("tp"),
            P("tp"),
            P("tp", None),
            P("tp", None),
        ),
        out_specs=P("sp", "tp"),
        check_vma=False,
    )
```

profile of v0, /device:TPU:504, one launch (start us, length us, event | category | flops | bytes accessed | tf_op | source)
XLA Modules:
  0.0 481.0 jit_solution(1251563236978299214)
XLA Ops:
  9.0 4.3 all-to-all-start
  13.4 21.5 %all-to-all-done = bf16[8,384,256]{1,2,0:T(8,128)(2,1)S(1)} async-done(((bf16[8,384,256]{1,2,0:T(8,128)(2,1)}), bf16[8,384,256]{1,2,0:T(8,128)(2,1)S(1)}, u32[]{:S(2)}, u32[]{:S(2)}) %all-to-all-start) | async-done | bytes 1572896 | tf_op jit(solution)/shard_map/all_to_all | solution.py:24
  54.0 5.3 %all-to-all-done.1 = f32[8,1,768]{2,1,0:T(1,128)S(1)} async-done(((f32[8,1,768]{2,1,0:T(1,128)}), f32[8,1,768]{2,1,0:T(1,128)S(1)}, u32[]{:S(2)}, u32[]{:S(2)}) %all-to-all-start.1) | async-done | bytes 24608 | tf_op jit(solution)/shard_map/all_to_all | solution.py:24
  59.5 109.1 %all-gather.2.cloned.1.call-done = bf16[24576,288]{0,1:T(8,128)(2,1)} async-done(((bf16[384,288]{0,1:T(8,128)(2,1)}), bf16[24576,288]{0,1:T(8,128)(2,1)}) %all-gather.2.cloned.1.call-update) | async-done | bytes 14155792 | tf_op jit(solution)/shard_map/all_gather | solution.py:40
  171.3 10.4 %fusion.60 = (bf16[24576,128]{0,1:T(8,128)(2,1)}, bf16[24576,128]{0,1:T(8,128)(2,1)}) fusion(bf16[24576,288]{0,1:T(8,128)(2,1)} %all-gather.2.cloned.1.call-done), kind=kLoop, calls=%fused_computation.197 | loop fusion | bytes 25165824 | tf_op jit(solution)/shard_map/slice | solution.py:42
  181.8 255.8 %while.15 = (s32[]{:T(128)}, f32[2,384]{1,0:T(2,128)S(1)}, f32[2,384]{1,0:T(2,128)S(1)}, f32[384,2,64]{0,2,1:T(8,128)S(1)}, s32[48]{0:T(128)S(1)}, /*index=5*/s3...) while((s32[]{:T(128)}, f32[2,384]{1,0:T(2,128)S(1)}, ...), condition=%wide.region_7.8_spmd.clone, body=%wide.region_2.7_spmd.clone.sunk | while | flops 130059392 | bytes 10070389 | solution.py:230
  183.0 4.1 conditional.3
  193.7 4.0 conditional.3
  199.0 4.0 conditional.3
  204.4 4.0 conditional.3
  209.7 4.0 conditional.3
  215.0 4.0 conditional.3
  220.4 4.0 conditional.3
  225.7 4.0 conditional.3
  231.0 4.0 conditional.3
  236.4 4.0 conditional.3
  241.7 4.0 conditional.3
  247.0 4.0 conditional.3
  252.3 4.0 conditional.3
  257.7 4.0 conditional.3
  263.0 4.0 conditional.3
  268.3 4.0 conditional.3
  273.7 4.0 conditional.3
  279.0 4.0 conditional.3
  284.3 4.0 conditional.3
  289.7 4.0 conditional.3
  295.0 4.0 conditional.3
  300.3 4.0 conditional.3
  305.6 4.0 conditional.3
  311.0 4.0 conditional.3
  316.3 4.0 conditional.3
  321.6 4.0 conditional.3
  327.0 4.0 conditional.3
  332.3 4.0 conditional.3
  337.6 4.0 conditional.3
  343.0 4.0 conditional.3
  348.3 4.0 conditional.3
  353.6 4.0 conditional.3
  359.0 4.0 conditional.3
  364.3 4.0 conditional.3
  369.6 4.0 conditional.3
  374.9 4.0 conditional.3
  380.3 4.0 conditional.3
  385.6 4.0 conditional.3
  390.9 4.0 conditional.3
  396.3 4.0 conditional.3
  437.7 9.5 %all_to_all.22 = f32[8,1,768]{2,1,0:T(1,128)S(1)} all-to-all(f32[8,1,768]{2,1,0:T(1,128)S(1)} %broadcast_in_dim.82), channel_id=1, replica_groups=mesh['sp'=64,'tp'=8] {'tp'}, dimensions={0} | all-to-all | bytes 49152 | tf_op jit(solution)/shard_map/all_to_all | solution.py:24
  449.2 24.0 %all_to_all.23 = bf16[8,256,384]{1,2,0:T(8,128)(2,1)S(1)} all-to-all(bf16[8,256,384]{1,2,0:T(8,128)(2,1)S(1)} %bitcast.126), channel_id=1, replica_groups=mesh['sp'=64,'tp'=8] {'tp'}, dimensions={0} | all-to-all | bytes 3145728 | tf_op jit(solution)/shard_map/all_to_all | solution.py:75
  (717 shorter events, 278.2 us)
Async XLA Ops:
  6.5 31.3 %copy-start = (bf16[2048,256]{1,0:T(8,128)(2,1)S(1)}, bf16[2048,256]{1,0:T(8,128)(2,1)}, u32[]{:S(2)}) copy-start(bf16[2048,256]{1,0:T(8,128)(2,1)} %param.26) | copy-start | bytes 3145732
  9.0 25.9 %all-to-all-start = ((bf16[8,384,256]{1,2,0:T(8,128)(2,1)}), bf16[8,384,256]{1,2,0:T(8,128)(2,1)S(1)}, u32[]{:S(2)}, u32[]{:S(2)}) async-start(bf16[8,384,256]{1,2,0:T(8,128)(2,1)} %broadcast_in_dim.48), calls=%async_computation | async-start | bytes 3145728 | tf_op jit(solution)/shard_map/all_to_all | solution.py:24
  13.3 22.7 %copy-start.9 = (f32[2048]{0:T(1024)S(1)}, f32[2048]{0:T(1024)}, u32[]{:S(2)}) copy-start(f32[2048]{0:T(1024)} %param.23) | copy-start | bytes 24580
  13.3 155.3 %all-gather.2.cloned.1.call-start = ((), (), s32[]{:S(2)}) async-start(), calls=%async_computation.4 | async-start | bytes 14376960 | tf_op jit(solution)/shard_map/all_gather | solution.py:40
  34.9 1.2 copy-start.1
  37.8 0.8 copy-start.6
  37.8 0.8 copy-start.10
  37.8 1.1 copy-start.7
  37.8 1.4 copy-start.5
  38.9 1.6 copy-start.8
  38.9 1.6 copy-start.15
  40.5 1.0 copy-start.16
  41.6 2.0 copy-start.4
  42.1 1.9 copy-start.17
  42.2 5.9 %collective-permute-start = (bf16[30,128]{0,1:T(8,128)(2,1)S(1)}, bf16[30,128]{0,1:T(8,128)(2,1)S(1)}, u32[]{:S(2)}, u32[]{:S(2)}) collective-permute-start(bf16[30,128]{0,1:T(8,128)(2,1)S(1)} %slice.299), channel_id=1, source_target_pairs={{0,8},{8,16},{16,24},{24,32},{32,40},{40,48},{48,56},{56,64},{64,7... | collective-permute-start | bytes 23048 | tf_op jit(solution)/shard_map/ppermute | solution.py:50
  44.0 15.4 %copy-start.11 = (f32[128]{0:T(128)S(1)}, f32[128]{0:T(128)}, u32[]{:S(2)}) copy-start(f32[128]{0:T(128)} %param.35) | copy-start | bytes 1540
  44.0 15.4 %copy-start.12 = (f32[128]{0:T(128)S(1)}, f32[128]{0:T(128)}, u32[]{:S(2)}) copy-start(f32[128]{0:T(128)} %param.34) | copy-start | bytes 1540
  50.6 8.7 %all-to-all-start.1 = ((f32[8,1,768]{2,1,0:T(1,128)}), f32[8,1,768]{2,1,0:T(1,128)S(1)}, u32[]{:S(2)}, u32[]{:S(2)}) async-start(f32[8,1,768]{2,1,0:T(1,128)} %broadcast_in_dim.49), calls=%async_computation.1 | async-start | bytes 49152 | tf_op jit(solution)/shard_map/all_to_all | solution.py:24
  181.7 265.4 %copy-start.13 = (f32[128]{0:T(128)S(1)}, f32[128]{0:T(128)}, u32[]{:S(2)}) copy-start(f32[128]{0:T(128)} %param.36) | copy-start | bytes 1540
  181.8 265.5 %copy-start.2 = (bf16[128,2048]{1,0:T(8,128)(2,1)S(1)}, bf16[128,2048]{1,0:T(8,128)(2,1)}, u32[]{:S(2)}) copy-start(bf16[128,2048]{1,0:T(8,128)(2,1)} %param.38) | copy-start | bytes 1572868
  447.3 1.0 copy-start.3
  447.3 1.0 copy-start.14
Sparse Core Ops, SparseCore 0:
  40.6 127.9 all-gather.1
where the time goes:
time: 486 us; the launch traced here: 481 us
  waiting for transfers between devices  139 us (29%)
  matrix products  115 us (24%)
  local copies, waits for them, and re-layouts  102 us (21%)
  loops' own time  37.1 us (8%)
  blocking collectives  33.5 us (7%)
  other arithmetic  31.7 us (7%)
  between operations  13.9 us (3%)
  starting transfers between devices  9.1 us (2%)
    all_gather x1, waiting for transfers between devices, sent_together(): lax.all_gather(both, axis, axis=dim, tiled=True)  109 us
    dot_general x48, matrix products, attend(): jnp.einsum('qhd,kd->hqk', query_rot, rot_block, preferred_element_type=jn...  59.7 us
    dynamic_slice x48, local copies, waits for them, and re-layouts, visit_block(): lax.dynamic_slice_in_dim(member, start_row, step_len, 0)  55 us
    another operation x1, loops' own time, shards(): lax.scan(visit_block, start_state, jnp.arange(piece_rows // step_len, dty...  33.2 us
    dynamic_slice x48, local copies, waits for them, and re-layouts, shards(): lax.scan(visit_block, start_state, jnp.arange(piece_rows // step_len, dty...  28.1 us
    all_to_all x2, waiting for transfers between devices, copy_for_each(): lax.all_to_all(jnp.broadcast_to(x[None], (peers, *x.shape)), axis, 0, 0,...  26.8 us
    dot_general x48, matrix products, attend(): jnp.einsum('qhd,khd->hqk', queries, key_block, preferred_element_type=jnp...  26.7 us
    all_to_all x1, blocking collectives, summed_on_arrival(): lax.all_to_all(pieces, axis, split_axis=0, concat_axis=0, tiled=True)  24 us
  transfers between devices with their start and end apart: 4, of which 4 were waited for; matrix products, arithmetic and copies ran while one was open for 1% of the time, Pallas kernels for 0%

commit v1 on v0

--- a/solution.py
+++ b/solution.py
@@ -3,6 +3,8 @@
 import jax
 import jax.numpy as jnp
 from jax import lax
+from jax.experimental import pallas as pl
+from jax.experimental.pallas import tpu as pltpu
 from jax.sharding import PartitionSpec as P
 
 D_MODEL = 2048
@@ -93,6 +95,320 @@
         ],
         axis=-1,
     )
+
+MESH = pl.DeviceIdType.MESH
+ROWS = 384
+SHARE = 112
+KSETS = 16
+LOG2E = 1.4426950408889634
+
+
+def ring_peers(tp):
+    x, c = tp // 2, tp % 2
+    right = ((x + 1) % 4) * 2 + c
+    left = ((x + 3) % 4) * 2 + c
+    far = ((x + 2) % 4) * 2 + c
+    partner = x * 2 + (1 - c)
+    return right, left, far, partner
+
+
+class RingGather:
+    def __init__(self, buf, lo, hi, mid, send, recv, sp, tp):
+        self.buf, self.lo, self.hi, self.mid = buf, lo, hi, mid
+        self.send, self.recv, self.sp, self.tp = send, recv, sp, tp
+        self.right, self.left, self.far, self.partner = ring_peers(tp)
+
+    def piece(self, slot, part=None):
+        lo, hi = {None: (self.lo, self.hi), 0: (self.lo, self.mid), 1: (self.mid, self.hi)}[part]
+        return self.buf.at[slot, pl.ds(lo, hi - lo)]
+
+    def copy(self, slot, part, sem, to):
+        return pltpu.make_async_remote_copy(
+            src_ref=self.piece(slot, part),
+            dst_ref=self.piece(slot, part),
+            send_sem=self.send.at[sem],
+            recv_sem=self.recv.at[sem],
+            device_id=(self.sp, to),
+            device_id_type=MESH,
+        )
+
+    def begin(self):
+        self.copy(self.tp, None, 0, self.right).start()
+        self.copy(self.tp, None, 1, self.left).start()
+        self.copy(self.tp, None, 2, self.partner).start()
+
+    def relay(self):
+        self.copy(self.left, None, 0, self.right).wait_recv()
+        self.copy(self.left, 0, 5, self.right).start()
+        self.copy(self.left, None, 3, self.partner).start()
+        self.copy(self.right, None, 1, self.left).wait_recv()
+        self.copy(self.right, 1, 6, self.left).start()
+        self.copy(self.right, None, 4, self.partner).start()
+
+    def relay_far(self):
+        self.copy(self.far, 0, 5, self.right).wait_recv()
+        self.copy(self.far, 0, 7, self.partner).start()
+        self.copy(self.far, 1, 6, self.left).wait_recv()
+        self.copy(self.far, 1, 8, self.partner).start()
+
+    def finish(self):
+        for sem, part in ((2, None), (3, None), (4, None), (7, 0), (8, 1)):
+            self.copy(self.far, part, sem, self.partner).wait_recv()
+
+    def drain(self):
+        for sem, part in ((0, None), (1, None), (2, None), (3, None), (4, None), (5, 0), (6, 1), (7, 0), (8, 1)):
+            self.copy(self.tp, part, sem, self.partner).wait_send()
+
+
+def member_z(member, kind):
+    return 2 * member + (kind + member) % 2
+
+
+def attention_kernel(
+    q_ref, share_ref, key_up_ref, value_up_ref, out_ref,
+    qbuf, kbuf, kk, vv, wkv, top, acc, o_send, l_send, o_recv, l_recv, own_lse,
+    q_ssem, q_rsem, k_ssem, k_rsem, ag_ssem, ag_rsem, o_ssem, o_rsem, l_ssem, l_rsem,
+):
+    sp, tp = lax.axis_index("sp"), lax.axis_index("tp")
+    z, y = sp // 8, sp % 8
+    kind, mine = (z + z // 2) % 2, z // 2
+    right, left, far, partner = ring_peers(tp)
+
+    members = [None]
+    for i in range(1, 4):
+        members.append(member_z((mine + i) % 4, kind) * 8 + y)
+    key_peers = []
+    for dz in range(8):
+        zz = (z + dz) % 8
+        for e in range(2):
+            yy = (y % 4 + z // 2 + 4 - zz // 2) % 4
+            yy = (yy + 4 * (y // 4) + 4 * e) % 8
+            key_peers.append(zz * 8 + yy)
+
+    barrier = pltpu.get_barrier_semaphore()
+    for i in range(1, 4):
+        pl.semaphore_signal(barrier, inc=1, device_id=(members[i], tp), device_id_type=MESH)
+    for i in range(1, 16):
+        pl.semaphore_signal(barrier, inc=1, device_id=(key_peers[i], tp), device_id_type=MESH)
+    for peer in (right, left, partner):
+        pl.semaphore_signal(barrier, inc=1, device_id=(sp, peer), device_id_type=MESH)
+    pl.semaphore_wait(barrier, 21)
+
+    slot = z * 2 + y // 4
+    half = z // 4
+
+    def key_copy(i):
+        return pltpu.make_async_remote_copy(
+            src_ref=share_ref,
+            dst_ref=kbuf.at[tp, slot],
+            send_sem=k_ssem.at[i],
+            recv_sem=k_rsem.at[half],
+            device_id=(key_peers[i], tp),
+            device_id_type=MESH,
+        )
+
+    def query_copy(i):
+        return pltpu.make_async_remote_copy(
+            src_ref=q_ref,
+            dst_ref=qbuf.at[i - 1],
+            send_sem=q_ssem.at[i - 1],
+            recv_sem=q_rsem.at[i - 1],
+            device_id=(members[i], tp),
+            device_id_type=MESH,
+        )
+
+    own_copy = pltpu.make_async_copy(share_ref, kbuf.at[tp, slot], k_rsem.at[half])
+    own_copy.start()
+    for i in range(1, 16):
+        key_copy(i).start()
+    for i in range(1, 4):
+        query_copy(i).start()
+
+    lane = lax.broadcasted_iota(jnp.int32, (256, 128), 1)
+    for n, ref in enumerate((key_up_ref, value_up_ref)):
+        w = ref[...].astype(jnp.float32)
+        wkv[:, pl.ds(256 * n, 128)] = jnp.where(lane < 64, w, 0.0).astype(jnp.bfloat16)
+        wkv[:, pl.ds(256 * n + 128, 128)] = jnp.where(
+            lane < 64, pltpu.roll(w, 64, 1), 0.0
+        ).astype(jnp.bfloat16)
+
+    gathers = []
+    for p in range(2):
+        arrived = kbuf.at[tp, pl.ds(8 * p, 8)]
+        pltpu.make_async_copy(arrived, arrived, k_rsem.at[p]).wait()
+        gather = RingGather(
+            kbuf, 8 * p, 8 * p + 8, 8 * p + 4, ag_ssem.at[p], ag_rsem.at[p], sp, tp
+        )
+        gather.begin()
+        gathers.append(gather)
+    for gather in gathers:
+        gather.relay()
+
+    low = lax.broadcasted_iota(jnp.int32, (ROWS, 128), 1) < 64
+
+    def assemble(s, carry):
+        first = kbuf[:, s, 0:48, :].reshape(ROWS, 128)
+        second = kbuf[:, s, 48:96, :].reshape(ROWS, 128)
+        rows = jnp.concatenate([first, second], axis=1)
+        product = jnp.dot(rows, wkv[...], preferred_element_type=jnp.float32)
+        folded = kbuf[0:6, s, 96:112, :].astype(jnp.float32).reshape(96, 128)
+        turned = [pltpu.roll(folded, (64 - 32 * j) % 128, 1).reshape(6, 1, 16, 128) for j in range(4)]
+        rotary = jnp.concatenate(turned, axis=1).reshape(ROWS, 128)
+        at = pl.ds(pl.multiple_of(s * ROWS, ROWS), ROWS)
+        for h in range(2):
+            kk[h, at, :] = jnp.where(low, product[:, 128 * h : 128 * h + 128], rotary).astype(jnp.bfloat16)
+            vv[h, at, :] = jnp.where(
+                low, product[:, 256 + 128 * h : 384 + 128 * h], 1.0
+            ).astype(jnp.bfloat16)
+        return carry
+
+    for p in range(2):
+        gathers[p].relay_far()
+    for p in range(2):
+        gathers[p].finish()
+        lax.fori_loop(8 * p, 8 * p + 8, assemble, 0)
+
+    def step(queries, start, size, diagonal):
+        for h in range(2):
+            at = pl.ds(pl.multiple_of(start, ROWS), size)
+            scores = lax.dot_general(
+                queries[:, 128 * h : 128 * h + 128],
+                kk[h, at, :],
+                (((1,), (1,)), ((), ())),
+                preferred_element_type=jnp.float32,
+            )
+            if diagonal:
+                seen = lax.broadcasted_iota(jnp.int32, (ROWS, size), 1) <= lax.broadcasted_iota(
+                    jnp.int32, (ROWS, size), 0
+                )
+                scores = jnp.where(seen, scores, far_below)
+            before = top[h]
+            now = jnp.maximum(before, jnp.max(scores, axis=1, keepdims=True))
+            top[h] = now
+            weights = jnp.exp2(scores - now[:, :1]).astype(jnp.bfloat16)
+            acc[h] = acc[h] * jnp.exp2(before - now) + jnp.dot(
+                weights, vv[h, at, :], preferred_element_type=jnp.float32
+            )
+
+    def attend(queries, whole, diagonal):
+        top[...] = jnp.full(top.shape, far_below, jnp.float32)
+        acc[...] = jnp.zeros(acc.shape, jnp.float32)
+
+        def pair(j, carry):
+            step(queries, j * (2 * ROWS), 2 * ROWS, False)
+            return carry
+
+        lax.fori_loop(0, whole // 2, pair, 0)
+
+        @pl.when(whole % 2 == 1)
+        def _():
+            step(queries, (whole - 1) * ROWS, ROWS, False)
+
+        if diagonal:
+            step(queries, whole * ROWS, ROWS, True)
+        sums, tops = [], []
+        for h in range(2):
+            a = acc[h]
+            total = jnp.where(low, pltpu.roll(a, 64, 1), a)
+            sums.append(total)
+            tops.append(top[h] + jnp.log2(jnp.maximum(total, 1e-37)))
+        value = jnp.where(low, acc[0], pltpu.roll(acc[1], 64, 1))
+        total = jnp.where(low, sums[0], sums[1])
+        return value / jnp.maximum(total, 1e-37), tops
+
+    tag = lax.broadcasted_iota(jnp.int32, (ROWS, 128), 1)
+
+    def back_copies(i):
+        return (
+            pltpu.make_async_remote_copy(
+                src_ref=o_send.at[i - 1],
+                dst_ref=o_recv.at[i - 1],
+                send_sem=o_ssem.at[i - 1],
+                recv_sem=o_rsem.at[i - 1],
+                device_id=(member_z((mine + 4 - i) % 4, kind) * 8 + y, tp),
+                device_id_type=MESH,
+            ),
+            pltpu.make_async_remote_copy(
+                src_ref=l_send.at[i - 1],
+                dst_ref=l_recv.at[i - 1],
+                send_sem=l_ssem.at[i - 1],
+                recv_sem=l_rsem.at[i - 1],
+                device_id=(member_z((mine + 4 - i) % 4, kind) * 8 + y, tp),
+                device_id_type=MESH,
+            ),
+        )
+
+    residue = (y + mine) % 4
+    for i in (2, 1, 3):
+        query_copy(i).wait_recv()
+        their = (mine + 4 - i) % 4
+        their_z = member_z(their, kind)
+        first = (residue + 4 - their) % 4
+        whole = (
+            2 * their_z
+            + jnp.where(first <= y, 1, 0).astype(jnp.int32)
+            + jnp.where(first + 4 <= y, 1, 0).astype(jnp.int32)
+        )
+        out, tops = attend(qbuf.at[i - 1], whole, False)
+        o_send[i - 1] = out.astype(jnp.bfloat16)
+        packed = jnp.where(tag < 4, tops[0], tops[1])
+        l_send[i - 1] = jnp.transpose(packed)[0:8, :]
+        for copy in back_copies(i):
+            copy.start()
+    out, tops = attend(q_ref, 2 * z + y // 4, True)
+    own_lse[...] = jnp.where(low, tops[0], tops[1])
+
+    logs, values = [own_lse[...]], [out]
+    for i in range(1, 4):
+        for copy in back_copies(i):
+            copy.wait_recv()
+        columns = jnp.transpose(l_recv[i - 1])
+        logs.append(jnp.where(low, columns[:, 0:1], columns[:, 4:5]))
+        values.append(o_recv[i - 1].astype(jnp.float32))
+    peak = jnp.maximum(jnp.maximum(logs[0], logs[1]), jnp.maximum(logs[2], logs[3]))
+    shares = [jnp.exp2(log - peak) for log in logs]
+    total = shares[0] + shares[1] + shares[2] + shares[3]
+    merged = sum(s * v for s, v in zip(shares, values))
+    out_ref[...] = (merged / total).astype(jnp.bfloat16)
+
+    for i in range(1, 16):
+        key_copy(i).wait_send()
+    for i in range(1, 4):
+        query_copy(i).wait_send()
+        for copy in back_copies(i):
+            copy.wait_send()
+    for gather in gathers:
+        gather.drain()
+
+
+def attention(queries, share, key_up, value_up):
+    vmem = pl.BlockSpec(memory_space=pltpu.VMEM)
+    bf, f32 = jnp.bfloat16, jnp.float32
+    dma = pltpu.SemaphoreType.DMA
+    return pl.pallas_call(
+        attention_kernel,
+        out_shape=jax.ShapeDtypeStruct((ROWS, 128), bf),
+        in_specs=[vmem] * 4,
+        out_specs=vmem,
+        scratch_shapes=[
+            pltpu.VMEM((3, ROWS, 256), bf),
+            pltpu.VMEM((8, KSETS, SHARE, 128), bf),
+            pltpu.VMEM((2, KSETS * ROWS, 128), bf),
+            pltpu.VMEM((2, KSETS * ROWS, 128), bf),
+            pltpu.VMEM((256, 512), bf),
+            pltpu.VMEM((2, ROWS, 128), f32),
+            pltpu.VMEM((2, ROWS, 128), f32),
+            pltpu.VMEM((3, ROWS, 128), bf),
+            pltpu.VMEM((3, 8, ROWS), f32),
+            pltpu.VMEM((3, ROWS, 128), bf),
+            pltpu.VMEM((3, 8, ROWS), f32),
+            pltpu.VMEM((ROWS, 128), f32),
+            dma((3,)), dma((3,)), dma((16,)), dma((2,)), dma((2, 9)), dma((2, 9)),
+            dma((3,)), dma((3,)), dma((3,)), dma((3,)),
+        ],
+        compiler_params=pltpu.CompilerParams(collective_id=1, has_side_effects=True),
+        name="attention",
+    )(queries, share, key_up, value_up)
 
 
 def shards(
@@ -139,12 +455,6 @@
     row_scale = lax.rsqrt(square_sum / D_MODEL + norm_eps)[:, None]
     positions = lax.axis_index("sp") * tok_rows + jnp.arange(tok_rows, dtype=jnp.int32)
     cos_table, sine_table = rotary_tables(positions, ROT_DIM // 2)
-    queries = (q_acc * row_scale).astype(jnp.bfloat16).reshape(tok_rows, heads_here, NOPE_DIM)
-    query_rot = rotate_half(
-        (qrot_acc * row_scale).reshape(tok_rows, heads_here, ROT_DIM),
-        cos_table[:, None, :],
-        sine_table[:, None, :],
-    ).astype(jnp.bfloat16)
     latent = (
         latent_raw
         * lax.rsqrt(jnp.mean(latent_raw * latent_raw, axis=1, keepdims=True) + norm_eps)
@@ -154,37 +464,22 @@
     gated_input = (value_acc * row_scale * jax.nn.sigmoid(gate_acc * row_scale)).astype(
         jnp.bfloat16
     )
-    query_end = (lax.axis_index("sp") + 1) * tok_rows
-    inv_scale = 1.0 / math.sqrt(NOPE_DIM + ROT_DIM)
-
-    def attend(carried, key_block, rot_block, value_block, key_offset):
-        run_max, run_sum, run_acc = carried
-        block_len = key_block.shape[0]
-        scores = (
-            jnp.einsum("qhd,khd->hqk", queries, key_block, preferred_element_type=jnp.float32)
-            + jnp.einsum("qhd,kd->hqk", query_rot, rot_block, preferred_element_type=jnp.float32)
-        ) * inv_scale
-        key_pos = key_offset + jnp.arange(block_len, dtype=jnp.int32)
-        visible = (key_pos[None, :] <= positions[:, None])[None]
-        new_max = jnp.maximum(run_max, jnp.max(jnp.where(visible, scores, far_below), axis=2))
-        exp_scores = jnp.where(visible, jnp.exp(scores - new_max[:, :, None]), 0.0)
-        shrink = jnp.exp(run_max - new_max)
-        run_sum = run_sum * shrink + jnp.sum(exp_scores, axis=2)
-        run_acc = run_acc * shrink.T[:, :, None] + jnp.einsum(
-            "hqk,khd->qhd",
-            exp_scores.astype(jnp.bfloat16),
-            value_block,
-            preferred_element_type=jnp.float32,
-        )
-        return (new_max, run_sum, run_acc)
-
-    def reshape_heads(sliced):
-        key_rows, value_rows, rot_block = sliced
-        return (
-            key_rows.reshape(-1, heads_here, NOPE_DIM),
-            value_rows.reshape(-1, heads_here, VALUE_DIM),
-            rot_block,
-        )
+    scale = LOG2E / math.sqrt(NOPE_DIM + ROT_DIM)
+    q_rot = rotate_half(
+        (qrot_acc * row_scale).reshape(tok_rows, heads_here, ROT_DIM),
+        cos_table[:, None, :],
+        sine_table[:, None, :],
+    )
+    q_nope = (q_acc * row_scale).reshape(tok_rows, heads_here, NOPE_DIM)
+    packed_queries = (
+        jnp.concatenate([q_nope, q_rot, jnp.zeros((tok_rows, heads_here, 32), jnp.float32)], axis=2)
+        * scale
+    ).astype(jnp.bfloat16).reshape(tok_rows, 256)
+    t = lax.axis_index("tp")
+    mine = lax.dynamic_slice_in_dim(latent, t * 48, 48, 0)
+    folds = key_rot.reshape(6, 4, 16, 32).transpose(0, 2, 1, 3).reshape(6, 16, 128)
+    fold = lax.dynamic_index_in_dim(folds, jnp.minimum(t, 5), 0, keepdims=False)
+    share = jnp.concatenate([mine[:, :128], mine[:, 128:], fold], axis=0)
 
     def square_rows(matrix):
         wide_rows = matrix.astype(jnp.float32)
@@ -204,38 +499,7 @@
     spread = moment_two / CONV_CH - mean_val * mean_val
     normed = (conv_out - mean_val[:, None]) * lax.rsqrt(spread + norm_eps)[:, None]
     swished = jax.nn.silu(normed * conv_ln_gain[None, :] + conv_ln_bias[None, :])
-    start_state = (
-        jnp.full((heads_here, tok_rows), far_below, jnp.float32),
-        jnp.zeros((heads_here, tok_rows), jnp.float32),
-        jnp.zeros((tok_rows, heads_here, VALUE_DIM), jnp.float32),
-    )
-    own_keys = jnp.dot(latent, key_up, preferred_element_type=jnp.float32).astype(jnp.bfloat16)
-    own_values = jnp.dot(latent, value_up, preferred_element_type=jnp.float32).astype(jnp.bfloat16)
-    pieces = sent_together((own_keys, own_values, key_rot), "sp", 0, 1)
-    piece_rows = pieces[0].shape[0]
-    step_len = math.gcd(piece_rows, 512)
-
-    def visit_block(running, block_idx):
-        start_row = block_idx * step_len
-        sliced = tuple(
-            (lax.dynamic_slice_in_dim(member, start_row, step_len, 0) for member in pieces)
-        )
-
-        def compute(current):
-            key_block, value_block, rot_block = reshape_heads(sliced)
-            return attend(current, key_block, rot_block, value_block, start_row)
-
-        return (lax.cond(start_row < query_end, compute, lambda current: current, running), None)
-
-    final_state = lax.scan(
-        visit_block, start_state, jnp.arange(piece_rows // step_len, dtype=jnp.int32)
-    )[0]
-    run_max, run_sum, run_acc = final_state
-    attended = (
-        (run_acc / run_sum.T[:, :, None])
-        .astype(jnp.bfloat16)
-        .reshape(tok_rows, heads_here * VALUE_DIM)
-    )
+    attended = attention(packed_queries, share, key_up, value_up)
     att_sq, conv_sq = in_one((square_rows(attended), square_rows(swished)), "tp")
     att_mixed = (
         attended.astype(jnp.float32)

time: 486 us -> 179 us (0.37)
  the two profiles are of different devices: /device:TPU:504 before, /device:TPU:120 now
where the time goes in v1:
time: 179 us
  Pallas kernels  88 us (49%)
  blocking collectives  31.8 us (18%)
  waiting for transfers between devices  24.5 us (14%)
  starting transfers between devices  11.2 us (6%)
  other arithmetic  8.7 us (5%)
  local copies, waits for them, and re-layouts  7.7 us (4%)
  matrix products  6.25 us (3%)
    pallas_call x1, Pallas kernels, attention(): pl.pallas_call(attention_kernel, out_shape=jax.ShapeDtypeStruct((ROWS, 12...  88 us
    all_to_all x2, waiting for transfers between devices, copy_for_each(): lax.all_to_all(jnp.broadcast_to(x[None], (peers, *x.shape)), axis, 0, 0,...  24.5 us
    all_to_all x1, blocking collectives, summed_on_arrival(): lax.all_to_all(pieces, axis, split_axis=0, concat_axis=0, tiled=True)  24 us
    all_to_all x2, starting transfers between devices, copy_for_each(): lax.all_to_all(jnp.broadcast_to(x[None], (peers, *x.shape)), axis, 0, 0,...  7.77 us
    all_to_all x1, blocking collectives, copy_for_each(): lax.all_to_all(jnp.broadcast_to(x[None], (peers, *x.shape)), axis, 0, 0,...  7.76 us
    dot_general x6, matrix products, add_product(): return jnp.dot(scaled, weight, preferred_element_type=jnp.float32)  3.98 us
  transfers between devices with their start and end apart: 3, of which 2 were waited for; matrix products, arithmetic and copies ran while one was open for 4% of the time, Pallas kernels for 49%

profile of v1, /device:TPU:120, one launch (start us, length us, event | category | flops | bytes accessed | tf_op | source)
XLA Modules:
  0.0 179.0 jit_solution(2643346901216546861)
XLA Ops:
  0.0 1.2 copy.56
  1.2 1.3 broadcast_in_dim.8
  2.5 4.4 %all-to-all-start = ((bf16[8,384,256]{1,2,0:T(8,128)(2,1)}), bf16[8,384,256]{1,2,0:T(8,128)(2,1)S(1)}, u32[]{:S(2)}, u32[]{:S(2)}) async-start(bf16[8,384,256]{1,2,0:T(8,128)(2,1)} %broadcast_in_dim.8), calls=%async_computation | async-start | bytes 3145728 | tf_op jit(solution)/shard_map/all_to_all | solution.py:26
  6.9 0.6 pad.14.clone
  7.6 0.7 slice_bitcast_fusion.30
  8.2 20.2 %all-to-all-done = bf16[8,384,256]{1,2,0:T(8,128)(2,1)S(1)} async-done(((bf16[8,384,256]{1,2,0:T(8,128)(2,1)}), bf16[8,384,256]{1,2,0:T(8,128)(2,1)S(1)}, u32[]{:S(2)}, u32[]{:S(2)}) %all-to-all-start) | async-done | bytes 1572896 | tf_op jit(solution)/shard_map/all_to_all | solution.py:26
  28.5 0.4 multiply_reduce_fusion
  28.9 0.7 copy-done.1
  29.7 1.8 fusion
  31.5 0.0 copy-start.4
  31.5 0.3 convolution_multiply_fusion.4
  31.8 0.2 subtract_convert_fusion
  32.0 0.1 concatenate.25
  32.1 0.1 concatenate.26
  32.3 0.2 maximum_bitcast_fusion
  32.4 0.2 copy.62
  32.6 0.1 reshape.121
  32.8 0.4 convolution_multiply_fusion.3
  33.1 0.1 copy.60
  33.3 0.1 copy.58
  33.4 1.6 convolution_multiply_fusion.1
  35.0 0.5 fusion.6
  35.6 0.1 slice.294
  35.6 3.5 %collective-permute-start = (bf16[30,128]{0,1:T(8,128)(2,1)S(1)}, bf16[30,128]{0,1:T(8,128)(2,1)S(1)}, u32[]{:S(2)}, u32[]{:S(2)}) collective-permute-start(bf16[30,128]{0,1:T(8,128)(2,1)S(1)} %slice.294), channel_id=1, source_target_pairs={{0,8},{8,16},{16,24},{24,32},{32,40},{40,48},{48,56},{56,64},{64,7... | collective-permute-start | bytes 23048 | tf_op jit(solution)/shard_map/ppermute | solution.py:52
  39.1 0.5 convolution_multiply_fusion.2
  39.7 0.7 multiply_reduce_fusion.1
  40.4 0.1 dynamic-slice
  40.4 0.1 fusion.47
  40.5 0.2 copy.61
  40.8 0.2 copy.73
  41.0 0.2 copy.72
  41.2 0.4 multiply_subtract_fusion
  41.8 0.9 fusion.7
  42.7 0.6 pad_maximum_fusion.1.share_ref
  43.3 0.7 copy.83
  44.0 88.0 %attention.1 = bf16[384,128]{1,0:T(8,128)(2,1)} custom-call(bf16[384,256]{1,0:T(8,128)(2,1)} %bitcast.105, bf16[112,128]{1,0:T(8,128)(2,1)} %pad_maximum_fusion.1.share_ref, bf16[256,128]{1,0:T(8,128)(2,1)} %key_up_ref.1, bf16[256,128]{1,0:T(8,128)(2,1)} %value_up_ref.1), custom_call_target="tpu_custom_call" | custom-call | tf_op jit(solution)/shard_map/attention/pallas_call | solution.py:388
  132.2 2.0 %fusion.48 = (f32[384]{0:T(512)S(1)}, f32[384]{0:T(512)S(1)}, f32[384,128]{0,1:T(8,128)S(1)}) fusion(bf16[384,128]{0,1:T(8,128)(2,1)S(1)} %fusion.6, f32[128]{0:T(128)S(1)} %get-tuple-element.45, bf16[30,128]{0,1:T(8,128)(2,1)S(1)} %collective-permute-done, f32[128]{0:T(128)S(1)} %get-tuple-element.46, f32[128]{0:T(128)S(1)} %copy-done.10, ...), kind=kLoop, calls=%fused_computation.176 | loop fusion | flops 9092352 | bytes 321536 | tf_op jit(solution)/shard_map/reduce_sum | solution.py:496
  134.2 0.6 broadcast_in_dim.10
  134.8 3.3 %all-to-all-start.1 = ((f32[8,1,768]{2,1,0:T(1,128)}), f32[8,1,768]{2,1,0:T(1,128)S(1)}, u32[]{:S(2)}, u32[]{:S(2)}) async-start(f32[8,1,768]{2,1,0:T(1,128)} %broadcast_in_dim.10), calls=%async_computation.1 | async-start | bytes 49152 | tf_op jit(solution)/shard_map/all_to_all | solution.py:26
  138.2 1.0 fusion.8
  139.2 4.3 %all-to-all-done.1 = f32[8,1,768]{2,1,0:T(1,128)S(1)} async-done(((f32[8,1,768]{2,1,0:T(1,128)}), f32[8,1,768]{2,1,0:T(1,128)S(1)}, u32[]{:S(2)}, u32[]{:S(2)}) %all-to-all-start.1) | async-done | bytes 24608 | tf_op jit(solution)/shard_map/all_to_all | solution.py:26
  143.6 0.2 multiply_reduce_fusion.2
  143.8 7.8 %all_to_all.22 = f32[8,1,768]{2,1,0:T(1,128)S(1)} all-to-all(f32[8,1,768]{2,1,0:T(1,128)S(1)} %broadcast_in_dim.11), channel_id=1, replica_groups=mesh['sp'=64,'tp'=8] {'tp'}, dimensions={0} | all-to-all | bytes 49152 | tf_op jit(solution)/shard_map/all_to_all | solution.py:26
  151.6 1.6 fusion.40
  153.2 0.7 add_convert_fusion
  153.9 0.1 copy.82
  154.0 24.0 %all_to_all.23 = bf16[8,256,384]{1,2,0:T(8,128)(2,1)S(1)} all-to-all(bf16[8,256,384]{1,2,0:T(8,128)(2,1)S(1)} %bitcast.102), channel_id=1, replica_groups=mesh['sp'=64,'tp'=8] {'tp'}, dimensions={0} | all-to-all | bytes 3145728 | tf_op jit(solution)/shard_map/all_to_all | solution.py:77
  178.0 0.9 reduce_sum.92
  (83 shorter events, 0.3 us)
Async XLA Ops:
  0.0 39.6 %copy-start = (bf16[2048,256]{1,0:T(8,128)(2,1)S(1)}, bf16[2048,256]{1,0:T(8,128)(2,1)}, u32[]{:S(2)}) copy-start(bf16[2048,256]{1,0:T(8,128)(2,1)} %param.22) | copy-start | bytes 3145732
  2.5 5.1 %copy-start.6 = (f32[31,128]{1,0:T(8,128)S(1)}, f32[31,128]{1,0:T(8,128)}, u32[]{:S(2)}) copy-start(f32[31,128]{1,0:T(8,128)} %param.29) | copy-start | bytes 47620
  2.5 26.0 %all-to-all-start = ((bf16[8,384,256]{1,2,0:T(8,128)(2,1)}), bf16[8,384,256]{1,2,0:T(8,128)(2,1)S(1)}, u32[]{:S(2)}, u32[]{:S(2)}) async-start(bf16[8,384,256]{1,2,0:T(8,128)(2,1)} %broadcast_in_dim.8), calls=%async_computation | async-start | bytes 3145728 | tf_op jit(solution)/shard_map/all_to_all | solution.py:26
  6.9 22.7 %copy-start.7 = (f32[2048]{0:T(1024)S(1)}, f32[2048]{0:T(1024)}, u32[]{:S(2)}) copy-start(f32[2048]{0:T(1024)} %param.19) | copy-start | bytes 24580
  28.5 1.2 copy-start.1
  29.6 1.8 %copy-start.5 = (bf16[2048,32]{0,1:T(8,128)(2,1)S(1)}, bf16[2048,32]{0,1:T(8,128)(2,1)}, u32[]{:S(2)}) copy-start(bf16[2048,32]{0,1:T(8,128)(2,1)} %param.23) | copy-start | bytes 393220
  31.5 1.3 copy-start.4
  33.4 1.6 copy-start.32
  35.0 4.1 %copy-start.33 = (bf16[2048,128]{1,0:T(8,128)(2,1)S(1)}, bf16[2048,128]{1,0:T(8,128)(2,1)}, u32[]{:S(2)}) copy-start(bf16[2048,128]{1,0:T(8,128)(2,1)} %param.20) | copy-start | bytes 1572868
  35.6 96.4 %collective-permute-start = (bf16[30,128]{0,1:T(8,128)(2,1)S(1)}, bf16[30,128]{0,1:T(8,128)(2,1)S(1)}, u32[]{:S(2)}, u32[]{:S(2)}) collective-permute-start(bf16[30,128]{0,1:T(8,128)(2,1)S(1)} %slice.294), channel_id=1, source_target_pairs={{0,8},{8,16},{16,24},{24,32},{32,40},{40,48},{48,56},{56,64},{64,7... | collective-permute-start | bytes 23048 | tf_op jit(solution)/shard_map/ppermute | solution.py:52
  39.6 0.8 copy-start.28
  40.7 1.1 copy-start.29
  41.6 90.5 %copy-start.10 = (f32[128]{0:T(128)S(1)}, f32[128]{0:T(128)}, u32[]{:S(2)}) copy-start(f32[128]{0:T(128)} %get-tuple-element.17) | copy-start | bytes 1540
  41.6 90.5 %copy-start.11 = (f32[128]{0:T(128)S(1)}, f32[128]{0:T(128)}, u32[]{:S(2)}) copy-start(f32[128]{0:T(128)} %get-tuple-element.18) | copy-start | bytes 1540
  41.6 90.5 %copy-start.12 = (f32[128]{0:T(128)S(1)}, f32[128]{0:T(128)}, u32[]{:S(2)}) copy-start(f32[128]{0:T(128)} %get-tuple-element.19) | copy-start | bytes 1540
  41.6 90.5 %copy-start.13 = (f32[128]{0:T(128)S(1)}, f32[128]{0:T(128)}, u32[]{:S(2)}) copy-start(f32[128]{0:T(128)} %get-tuple-element.20) | copy-start | bytes 1540
  41.6 90.5 %copy-start.14 = (f32[128]{0:T(128)S(1)}, f32[128]{0:T(128)}, u32[]{:S(2)}) copy-start(f32[128]{0:T(128)} %get-tuple-element.21) | copy-start | bytes 1540
  41.6 90.5 %copy-start.15 = (f32[128]{0:T(128)S(1)}, f32[128]{0:T(128)}, u32[]{:S(2)}) copy-start(f32[128]{0:T(128)} %get-tuple-element.22) | copy-start | bytes 1540
  41.7 90.5 %copy-start.16 = (f32[128]{0:T(128)S(1)}, f32[128]{0:T(128)}, u32[]{:S(2)}) copy-start(f32[128]{0:T(128)} %get-tuple-element.23) | copy-start | bytes 1540
  41.7 90.5 %copy-start.17 = (f32[128]{0:T(128)S(1)}, f32[128]{0:T(128)}, u32[]{:S(2)}) copy-start(f32[128]{0:T(128)} %get-tuple-element.24) | copy-start | bytes 1540
  41.7 90.5 %copy-start.18 = (f32[128]{0:T(128)S(1)}, f32[128]{0:T(128)}, u32[]{:S(2)}) copy-start(f32[128]{0:T(128)} %get-tuple-element.25) | copy-start | bytes 1540
  41.7 90.5 %copy-start.19 = (f32[128]{0:T(128)S(1)}, f32[128]{0:T(128)}, u32[]{:S(2)}) copy-start(f32[128]{0:T(128)} %get-tuple-element.26) | copy-start | bytes 1540
  41.7 90.5 %copy-start.20 = (f32[128]{0:T(128)S(1)}, f32[128]{0:T(128)}, u32[]{:S(2)}) copy-start(f32[128]{0:T(128)} %get-tuple-element.27) | copy-start | bytes 1540
  41.7 90.5 %copy-start.21 = (f32[128]{0:T(128)S(1)}, f32[128]{0:T(128)}, u32[]{:S(2)}) copy-start(f32[128]{0:T(128)} %get-tuple-element.28) | copy-start | bytes 1540
  41.7 90.5 %copy-start.22 = (f32[128]{0:T(128)S(1)}, f32[128]{0:T(128)}, u32[]{:S(2)}) copy-start(f32[128]{0:T(128)} %get-tuple-element.29) | copy-start | bytes 1540
  41.7 90.5 %copy-start.23 = (f32[128]{0:T(128)S(1)}, f32[128]{0:T(128)}, u32[]{:S(2)}) copy-start(f32[128]{0:T(128)} %get-tuple-element.30) | copy-start | bytes 1540
  41.7 90.5 %copy-start.24 = (f32[128]{0:T(128)S(1)}, f32[128]{0:T(128)}, u32[]{:S(2)}) copy-start(f32[128]{0:T(128)} %get-tuple-element.31) | copy-start | bytes 1540
  41.7 90.5 %copy-start.25 = (f32[128]{0:T(128)S(1)}, f32[128]{0:T(128)}, u32[]{:S(2)}) copy-start(f32[128]{0:T(128)} %get-tuple-element.32) | copy-start | bytes 1540
  41.8 90.5 %copy-start.26 = (f32[128]{0:T(128)S(1)}, f32[128]{0:T(128)}, u32[]{:S(2)}) copy-start(f32[128]{0:T(128)} %get-tuple-element.33) | copy-start | bytes 1540
  41.8 90.5 %copy-start.27 = (f32[128]{0:T(128)S(1)}, f32[128]{0:T(128)}, u32[]{:S(2)}) copy-start(f32[128]{0:T(128)} %get-tuple-element.34) | copy-start | bytes 1540
  41.8 101.8 %copy-start.8 = (f32[128]{0:T(128)S(1)}, f32[128]{0:T(128)}, u32[]{:S(2)}) copy-start(f32[128]{0:T(128)} %param.31) | copy-start | bytes 1540
  41.8 101.8 %copy-start.9 = (f32[128]{0:T(128)S(1)}, f32[128]{0:T(128)}, u32[]{:S(2)}) copy-start(f32[128]{0:T(128)} %param.30) | copy-start | bytes 1540
  41.8 109.8 %copy-start.2 = (bf16[128,2048]{1,0:T(8,128)(2,1)S(1)}, bf16[128,2048]{1,0:T(8,128)(2,1)}, u32[]{:S(2)}) copy-start(bf16[128,2048]{1,0:T(8,128)(2,1)} %param.34) | copy-start | bytes 1572868
  41.8 109.8 %copy-start.30 = (f32[128]{0:T(128)S(1)}, f32[128]{0:T(128)}, u32[]{:S(2)}) copy-start(f32[128]{0:T(128)} %param.32) | copy-start | bytes 1540
  134.8 8.7 %all-to-all-start.1 = ((f32[8,1,768]{2,1,0:T(1,128)}), f32[8,1,768]{2,1,0:T(1,128)S(1)}, u32[]{:S(2)}, u32[]{:S(2)}) async-start(f32[8,1,768]{2,1,0:T(1,128)} %broadcast_in_dim.10), calls=%async_computation.1 | async-start | bytes 49152 | tf_op jit(solution)/shard_map/all_to_all | solution.py:26
  151.6 1.6 copy-start.3
  151.6 1.6 copy-start.31

commit v2 on v0

v2 whole, which is shorter than its diff:
```python
import math

import jax
import jax.numpy as jnp
from jax import lax
from jax.experimental import pallas as pl
from jax.experimental.pallas import tpu as pltpu
from jax.sharding import PartitionSpec as P

D_MODEL = 2048
NOPE_DIM = 64
ROT_DIM = 32
VALUE_DIM = 64
CONV_CH = 1024
KERNEL = 31
ATT_WIDTH = 1024


norm_eps = 1e-06
far_below = -1e30
rope_base = 10000.0


def copy_for_each(x, axis):
    peers = lax.axis_size(axis)
    return lax.all_to_all(jnp.broadcast_to(x[None], (peers, *x.shape)), axis, 0, 0, tiled=True)


def in_order(pieces, dim):
    pieces = jnp.moveaxis(pieces, 0, dim)
    shape = pieces.shape
    return pieces.reshape(*shape[:dim], shape[dim] * shape[dim + 1], *shape[dim + 2 :])


def gathered_copies(x, axis, dim):
    pieces = copy_for_each(x, axis)
    return in_order(pieces, dim)


def rotary_tables(positions, half_dim):
    frequency = rope_base ** (-jnp.arange(half_dim, dtype=jnp.float32) / half_dim)
    angles = positions.astype(jnp.float32)[:, None] * frequency[None, :]
    return (jnp.cos(angles), jnp.sin(angles))


def rotate_half(values, cos_table, sine_table):
    half_dim = cos_table.shape[-1]
    front_half = values[..., :half_dim]
    back_half = values[..., half_dim:]
    return jnp.concatenate(
        [
            front_half * cos_table - back_half * sine_table,
            back_half * cos_table + front_half * sine_table,
        ],
        axis=-1,
    )


MESH = pl.DeviceIdType.MESH
ROWS = 384
SHARE = 112
KSETS = 16
PIECE = 4 * ROWS
LOG2E = 1.4426950408889634


def ring_peers(tp):
    x, c = tp // 2, tp % 2
    right = ((x + 1) % 4) * 2 + c
    left = ((x + 3) % 4) * 2 + c
    far = ((x + 2) % 4) * 2 + c
    partner = x * 2 + (1 - c)
    return right, left, far, partner


class RingGather:
    def __init__(self, buf, lo, hi, mid, send, recv, sp, tp):
        self.buf, self.lo, self.hi, self.mid = buf, lo, hi, mid
        self.send, self.recv, self.sp, self.tp = send, recv, sp, tp
        self.right, self.left, self.far, self.partner = ring_peers(tp)

    def piece(self, slot, part=None):
        lo, hi = {None: (self.lo, self.hi), 0: (self.lo, self.mid), 1: (self.mid, self.hi)}[part]
        return self.buf.at[slot, pl.ds(lo, hi - lo)]

    def copy(self, slot, part, sem, to):
        return pltpu.make_async_remote_copy(
            src_ref=self.piece(slot, part),
            dst_ref=self.piece(slot, part),
            send_sem=self.send.at[sem],
            recv_sem=self.recv.at[sem],
            device_id=(self.sp, to),
            device_id_type=MESH,
        )

    def begin(self):
        self.copy(self.tp, None, 0, self.right).start()
        self.copy(self.tp, None, 1, self.left).start()
        self.copy(self.tp, None, 2, self.partner).start()

    def relay(self):
        self.copy(self.left, None, 0, self.right).wait_recv()
        self.copy(self.left, 0, 5, self.right).start()
        self.copy(self.left, None, 3, self.partner).start()
        self.copy(self.right, None, 1, self.left).wait_recv()
        self.copy(self.right, 1, 6, self.left).start()
        self.copy(self.right, None, 4, self.partner).start()

    def relay_far(self):
        self.copy(self.far, 0, 5, self.right).wait_recv()
        self.copy(self.far, 0, 7, self.partner).start()
        self.copy(self.far, 1, 6, self.left).wait_recv()
        self.copy(self.far, 1, 8, self.partner).start()

    def finish(self):
        for sem, part in ((2, None), (3, None), (4, None), (7, 0), (8, 1)):
            self.copy(self.far, part, sem, self.partner).wait_recv()

    def drain(self):
        for sem, part in ((0, None), (1, None), (2, None), (3, None), (4, None), (5, 0), (6, 1), (7, 0), (8, 1)):
            self.copy(self.tp, part, sem, self.partner).wait_send()


def member_z(member, kind):
    return 2 * member + (kind + member) % 2


def layer_kernel(
    q_ref, share_ref, gated_ref, key_up_ref, value_up_ref, taps_ref, ln_gain_ref, ln_bias_ref,
    att_gain_ref, conv_gain_ref, att_w_ref, conv_w_ref, out_ref,
    qraw, qbuf, kbuf, kk, vv, wkv, top, acc, o_send, l_send, o_recv, l_recv, own_out, own_lse,
    halo, padded, conv_out, mom_send, mom_recv, cbuf, abuf, weights, gains, gain_all, branch,
    q_ssem, q_rsem, k_ssem, k_rsem, f_ssem, f_rsem, ag_ssem, ag_rsem, o_ssem, o_rsem, l_ssem, l_rsem,
    h_ssem, h_rsem, m_ssem, m_rsem, c_ssem, c_rsem, a_ssem, a_rsem, w_ssem, w_rsem, g_ssem, g_rsem,
    own_sem,
):
    sp, tp = lax.axis_index("sp"), lax.axis_index("tp")
    z, y = sp // 8, sp % 8
    kind, mine, parity = (z + z // 2) % 2, z // 2, y % 2
    residue = (y // 2 + mine) % 4
    bf, f32 = jnp.bfloat16, jnp.float32

    def member_sp(member):
        return member_z(member, kind) * 8 + y

    key_peers = []
    for dz in range(8):
        zz = (z + dz) % 8
        key_peers.append(zz * 8 + 2 * ((residue + 4 - zz // 2) % 4) + parity)
    pair = z * 8 + (y + 1 - 2 * parity)
    after, before_sp = (sp + 1) % 64, (sp + 63) % 64

    barrier = pltpu.get_barrier_semaphore()
    for i in range(1, 4):
        pl.semaphore_signal(
            barrier, inc=1, device_id=(member_sp((mine + i) % 4), tp), device_id_type=MESH
        )
    for i in range(1, 8):
        pl.semaphore_signal(barrier, inc=1, device_id=(key_peers[i], tp), device_id_type=MESH)
        pl.semaphore_signal(barrier, inc=1, device_id=(sp, (tp + i) % 8), device_id_type=MESH)
    pl.semaphore_signal(barrier, inc=1, device_id=(pair, tp), device_id_type=MESH)
    pl.semaphore_signal(barrier, inc=1, device_id=(before_sp, tp), device_id_type=MESH)
    pl.semaphore_wait(barrier, 19)

    def remote(src, dst, ssem, rsem, to):
        return pltpu.make_async_remote_copy(
            src_ref=src, dst_ref=dst, send_sem=ssem, recv_sem=rsem, device_id=to, device_id_type=MESH
        )

    halo_copy = remote(gated_ref.at[pl.ds(ROWS - 32, 32)], halo, h_ssem, h_rsem, (after, tp))
    halo_copy.start()

    slot = 4 * mine + 2 * parity + z % 2

    def key_copy(i):
        return remote(
            share_ref, kbuf.at[tp, slot], k_ssem.at[i], k_rsem.at[mine], (key_peers[i], tp)
        )

    pltpu.make_async_copy(share_ref, kbuf.at[tp, slot], k_rsem.at[mine]).start()
    for i in range(1, 8):
        key_copy(i).start()

    def query_copy(i):
        return remote(
            q_ref, qraw.at[i - 1], q_ssem.at[i - 1], q_rsem.at[i - 1], (member_sp((mine + i) % 4), tp)
        )

    for i in range(1, 4):
        query_copy(i).start()

    gains[...] = jnp.zeros(gains.shape, f32)
    gains[0:1, :] = att_gain_ref[...]
    gains[1:2, :] = conv_gain_ref[...]
    lane = lax.broadcasted_iota(jnp.int32, (256, 128), 1)
    for n, ref in enumerate((key_up_ref, value_up_ref)):
        w = ref[...].astype(f32)
        wkv[:, pl.ds(256 * n, 128)] = jnp.where(lane < 64, w, 0.0).astype(bf)
        wkv[:, pl.ds(256 * n + 128, 128)] = jnp.where(lane < 64, pltpu.roll(w, 64, 1), 0.0).astype(bf)

    tag = lax.broadcasted_iota(jnp.int32, (ROWS, 128), 1)
    low = tag < 64

    def unpack(ref, member):
        nope = ref[0:ROWS, :].astype(f32)
        fold = ref[ROWS : ROWS + ROWS // 2, :].astype(f32)
        for h in range(2):
            body = nope if h == 0 else pltpu.roll(nope, 64, 1)
            upper = pltpu.roll(fold, 64 - 32 * h, 1)
            lower = fold if h == 0 else pltpu.roll(fold, 96, 1)
            rotary = jnp.concatenate([upper, lower], axis=0)
            qbuf[member, h] = jnp.where(low, body, jnp.where(tag < 96, rotary, 0.0)).astype(bf)

    unpack(q_ref, mine)

    halo_copy.wait_recv()
    edge = halo[...].astype(f32)
    padded[0:32, :] = jnp.where(sp > 0, edge, jnp.zeros_like(edge))
    padded[pl.ds(32, ROWS), :] = gated_ref[...].astype(f32)
    total = jnp.zeros((ROWS, 128), f32)
    for tap in range(KERNEL):
        total = total + taps_ref[tap : tap + 1, :] * padded[pl.ds(tap + 2, ROWS), :]
    conv_out[...] = total
    sum_one = jnp.sum(total, axis=1, keepdims=True)
    sum_two = jnp.sum(total * total, axis=1, keepdims=True)
    mom_send[...] = jnp.transpose(jnp.where(tag == 0, sum_one, sum_two))[0:8, :]

    def forward(p):
        piece = kbuf.at[tp, pl.ds(4 * p + 2 * parity, 2)]
        return remote(piece, piece, f_ssem.at[p], f_rsem.at[p], (pair, tp))

    for p in range(4):
        piece = kbuf.at[tp, pl.ds(4 * p + 2 * parity, 2)]
        pltpu.make_async_copy(piece, piece, k_rsem.at[p]).wait()
        forward(p).start()

    def moment_copy(j):
        return remote(
            mom_send, mom_recv.at[tp], m_ssem.at[j], m_rsem.at[tp], (sp, (tp + j) % 8)
        )

    for j in range(1, 8):
        moment_copy(j).start()

    gathers = [
        RingGather(kbuf, 4 * p, 4 * p + 4, 4 * p + 2, ag_ssem.at[p], ag_rsem.at[p], sp, tp)
        for p in range(4)
    ]
    conv_gather = RingGather(cbuf, 0, ROWS, ROWS // 2, c_ssem, c_rsem, sp, tp)
    att_gather = RingGather(abuf, 0, ROWS, ROWS // 2, a_ssem, a_rsem, sp, tp)

    def begin(p):
        forward(p).wait_recv()
        gathers[p].begin()

    def assemble(p):
        slots = [4 * p + u for u in range(4)]
        first = jnp.concatenate([kbuf[:, s, 0:48, :].reshape(ROWS, 128) for s in slots], axis=0)
        second = jnp.concatenate([kbuf[:, s, 48:96, :].reshape(ROWS, 128) for s in slots], axis=0)
        product = jnp.dot(
            jnp.concatenate([first, second], axis=1), wkv[...], preferred_element_type=f32
        )
        pieces = []
        for s in slots:
            folded = kbuf[0:6, s, 96:112, :].astype(f32).reshape(96, 128)
            turned = [
                pltpu.roll(folded, (64 - 32 * j) % 128, 1).reshape(6, 1, 16, 128) for j in range(4)
            ]
            pieces.append(jnp.concatenate(turned, axis=1).reshape(ROWS, 128))
        rotary = jnp.concatenate(pieces, axis=0)
        front = lax.broadcasted_iota(jnp.int32, (PIECE, 128), 1) < 64
        for h in range(2):
            kk[h, pl.ds(p * PIECE, PIECE), :] = jnp.where(
                front, product[:, 128 * h : 128 * h + 128], rotary
            ).astype(bf)
            vv[h, pl.ds(p * PIECE, PIECE), :] = jnp.where(
                front, product[:, 256 + 128 * h : 384 + 128 * h], 1.0
            ).astype(bf)

    def step(member, p, masked):
        if masked:
            offset = lax.broadcasted_iota(jnp.int32, (ROWS, ROWS), 1) - lax.broadcasted_iota(
                jnp.int32, (ROWS, ROWS), 0
            )
            block = member_sp(member)
        for h in range(2):
            scores = lax.dot_general(
                qbuf[member, h],
                kk[h, pl.ds(p * PIECE, PIECE), :],
                (((1,), (1,)), ((), ())),
                preferred_element_type=f32,
            )
            if masked:
                columns = []
                for u in range(4):
                    key_block = (2 * p + u % 2) * 8 + 2 * ((residue + 4 - p) % 4) + u // 2
                    columns.append(
                        jnp.where(
                            offset <= (block - key_block) * ROWS,
                            scores[:, ROWS * u : ROWS * u + ROWS],
                            far_below,
                        )
                    )
                scores = jnp.concatenate(columns, axis=1)
            now = jnp.broadcast_to(jnp.max(scores, axis=1, keepdims=True), (ROWS, 128))
            if p > 0:
                before = top[member, h]
                now = jnp.maximum(before, now)
            top[member, h] = now
            likely = jnp.exp2(scores - jnp.concatenate([now] * (PIECE // 128), axis=1)).astype(bf)
            fresh = jnp.dot(likely, vv[h, pl.ds(p * PIECE, PIECE), :], preferred_element_type=f32)
            if p > 0:
                fresh = acc[member, h] * jnp.exp2(before - now) + fresh
            acc[member, h] = fresh

    def back_copies(member, source):
        to = (member_sp(member), tp)
        return (
            remote(o_send.at[member], o_recv.at[source], o_ssem.at[member], o_rsem.at[source], to),
            remote(l_send.at[member], l_recv.at[source], l_ssem.at[member], l_rsem.at[source], to),
        )

    def finalize(member):
        sums, tops = [], []
        for h in range(2):
            a = acc[member, h]
            part = jnp.where(low, pltpu.roll(a, 64, 1), a)
            sums.append(part)
            tops.append(top[member, h] + jnp.log2(part))
        value = jnp.where(low, acc[member, 0], pltpu.roll(acc[member, 1], 64, 1))
        value = value / jnp.where(low, sums[0], sums[1])
        o_send[member] = value.astype(bf)
        l_send[member] = jnp.transpose(jnp.where(tag < 4, tops[0], tops[1]))[0:8, :]

        @pl.when(mine == member)
        def _():
            own_out[...] = value
            own_lse[...] = jnp.where(low, tops[0], tops[1])

        @pl.when(mine != member)
        def _():
            for copy in back_copies(member, mine):
                copy.start()

    def weight_copies(j):
        to = (sp, (tp + j) % 8)
        columns = pl.ds(pl.multiple_of(256 * ((tp + j) % 8), 256), 256)
        return (
            remote(att_w_ref.at[:, columns], weights.at[0, tp], w_ssem.at[0, j], w_rsem.at[0, tp], to),
            remote(conv_w_ref.at[:, columns], weights.at[1, tp], w_ssem.at[1, j], w_rsem.at[1, tp], to),
            remote(gains, gain_all.at[tp], g_ssem.at[j], g_rsem.at[tp], to),
        )

    own_columns = pl.ds(pl.multiple_of(256 * tp, 256), 256)
    own_weights = (
        pltpu.make_async_copy(att_w_ref.at[:, own_columns], weights.at[0, tp], own_sem.at[0]),
        pltpu.make_async_copy(conv_w_ref.at[:, own_columns], weights.at[1, tp], own_sem.at[1]),
    )

    begin(0)
    gathers[0].relay()
    begin(1)
    gathers[0].relay_far()
    gathers[0].finish()
    assemble(0)
    gathers[1].relay()
    begin(2)
    step(mine, 0, True)
    gathers[1].relay_far()

    mom_recv[tp] = mom_send[...]
    for j in range(1, 8):
        source = (tp + j) % 8
        remote(mom_send, mom_recv.at[source], m_ssem.at[j], m_rsem.at[source], (sp, source)).wait_recv()
    moments = mom_recv[0]
    for t in range(1, 8):
        moments = moments + mom_recv[t]
    columns = jnp.transpose(moments)
    mean_val = columns[:, 0:1] / CONV_CH
    spread = columns[:, 1:2] / CONV_CH - mean_val * mean_val
    normed = (conv_out[...] - mean_val) * lax.rsqrt(spread + norm_eps)
    swished = jax.nn.silu(normed * ln_gain_ref[...] + ln_bias_ref[...])
    cbuf[tp] = swished.astype(bf)

    def arrive(i):
        query_copy(i).wait_recv()
        member = (mine + 4 - i) % 4
        unpack(qraw.at[i - 1], member)
        return member

    step(arrive(1), 0, True)
    gathers[2].relay()
    begin(3)
    step(arrive(3), 0, True)
    gathers[2].relay_far()
    gathers[3].relay()
    conv_gather.begin()
    for copy in own_weights:
        copy.start()
    step(arrive(2), 0, True)
    gathers[3].relay_far()
    conv_gather.relay()
    for j in range(1, 8):
        for copy in weight_copies(j):
            copy.start()
    finalize(0)
    gathers[1].finish()
    assemble(1)
    step(1, 1, True)
    conv_gather.relay_far()
    finalize(1)
    step(2, 1, False)
    step(3, 1, False)
    gathers[2].finish()
    assemble(2)
    step(2, 2, True)
    finalize(2)
    step(3, 2, False)
    gathers[3].finish()
    assemble(3)
    step(3, 3, True)
    finalize(3)

    gain_all[tp] = gains[...]
    conv_gather.finish()
    for copy in own_weights:
        copy.wait()
    for j in range(1, 8):
        source = (tp + j) % 8
        for n in range(2):
            remote(
                weights.at[n, source], weights.at[n, source], w_ssem.at[n, j], w_rsem.at[n, source], (sp, source)
            ).wait_recv()
        remote(gains, gain_all.at[source], g_ssem.at[j], g_rsem.at[source], (sp, source)).wait_recv()

    def product(buf, n):
        wide = jnp.concatenate([buf[t] for t in range(8)], axis=1).astype(f32)
        gain = jnp.concatenate([gain_all[t, n : n + 1, :] for t in range(8)], axis=1)
        power = jnp.sum(wide * wide, axis=1, keepdims=True)
        mixed = (wide * lax.rsqrt(power / CONV_CH + norm_eps) * gain).astype(bf)
        return jnp.dot(mixed, weights[n].reshape(1024, 256), preferred_element_type=f32)

    branch[...] = product(cbuf, 1)

    logs, values = [own_lse[...]], [own_out[...]]
    for i in range(1, 4):
        source = (mine + i) % 4
        for copy in back_copies(source, source):
            copy.wait_recv()
        columns = jnp.transpose(l_recv[source])
        logs.append(jnp.where(low, columns[:, 0:1], columns[:, 4:5]))
        values.append(o_recv[source].astype(f32))
    peak = jnp.maximum(jnp.maximum(logs[0], logs[1]), jnp.maximum(logs[2], logs[3]))
    shares = [jnp.exp2(log - peak) for log in logs]
    merged = sum(s * v for s, v in zip(shares, values)) / sum(shares)
    abuf[tp] = merged.astype(bf)

    att_gather.begin()
    att_gather.relay()
    att_gather.relay_far()
    att_gather.finish()
    out_ref[...] = (branch[...] + product(abuf, 0)).astype(bf)

    halo_copy.wait_send()
    for i in range(1, 8):
        key_copy(i).wait_send()
        moment_copy(i).wait_send()
        for copy in weight_copies(i):
            copy.wait_send()
    for p in range(4):
        forward(p).wait_send()
        gathers[p].drain()
    for i in range(1, 4):
        query_copy(i).wait_send()
        member = (mine + i) % 4
        for copy in back_copies(member, mine):
            copy.wait_send()
    conv_gather.drain()
    att_gather.drain()


def layer(*args):
    vmem, anywhere = pl.BlockSpec(memory_space=pltpu.VMEM), pl.BlockSpec(memory_space=pl.ANY)
    bf, f32 = jnp.bfloat16, jnp.float32
    dma = pltpu.SemaphoreType.DMA
    return pl.pallas_call(
        layer_kernel,
        out_shape=jax.ShapeDtypeStruct((ROWS, 256), bf),
        in_specs=[vmem] * 10 + [anywhere] * 2,
        out_specs=vmem,
        scratch_shapes=[
            pltpu.VMEM((3, ROWS + ROWS // 2, 128), bf),
            pltpu.VMEM((4, 2, ROWS, 128), bf),
            pltpu.VMEM((8, KSETS, SHARE, 128), bf),
            pltpu.VMEM((2, KSETS * ROWS, 128), bf),
            pltpu.VMEM((2, KSETS * ROWS, 128), bf),
            pltpu.VMEM((256, 512), bf),
            pltpu.VMEM((4, 2, ROWS, 128), f32),
            pltpu.VMEM((4, 2, ROWS, 128), f32),
            pltpu.VMEM((4, ROWS, 128), bf),
            pltpu.VMEM((4, 8, ROWS), f32),
            pltpu.VMEM((4, ROWS, 128), bf),
            pltpu.VMEM((4, 8, ROWS), f32),
            pltpu.VMEM((ROWS, 128), f32),
            pltpu.VMEM((ROWS, 128), f32),
            pltpu.VMEM((32, 128), bf),
            pltpu.VMEM((32 + ROWS, 128), f32),
            pltpu.VMEM((ROWS, 128), f32),
            pltpu.VMEM((8, ROWS), f32),
            pltpu.VMEM((8, 8, ROWS), f32),
            pltpu.VMEM((8, ROWS, 128), bf),
            pltpu.VMEM((8, ROWS, 128), bf),
            pltpu.VMEM((2, 8, 128, 256), bf),
            pltpu.VMEM((8, 128), f32),
            pltpu.VMEM((8, 8, 128), f32),
            pltpu.VMEM((ROWS, 256), f32),
            dma((3,)), dma((3,)), dma((8,)), dma((4,)), dma((4,)), dma((4,)), dma((4, 9)), dma((4, 9)),
            dma((4,)), dma((4,)), dma((4,)), dma((4,)), dma, dma, dma((8,)), dma((8,)),
            dma((9,)), dma((9,)), dma((9,)), dma((9,)), dma((2, 8)), dma((2, 8)), dma((8,)), dma((8,)),
            dma((2,)),
        ],
        compiler_params=pltpu.CompilerParams(collective_id=1, has_side_effects=True),
        name="layer",
    )(*args)


def shards(
    tokens,
    input_gain,
    query_weight,
    query_rot_weight,
    kv_down,
    rot_down,
    kv_gain,
    key_up,
    value_up,
    conv_value_weight,
    conv_gate_weight,
    conv_taps,
    conv_ln_gain,
    conv_ln_bias,
    att_out_gain,
    conv_out_gain,
    att_out_weight,
    conv_out_weight,
):
    tok_rows = tokens.shape[0]
    heads_here = key_up.shape[1] // NOPE_DIM
    weight_list = (
        query_weight,
        query_rot_weight,
        kv_down,
        rot_down,
        conv_value_weight,
        conv_gate_weight,
    )
    wide_part = gathered_copies(tokens, "tp", 1).astype(jnp.float32)
    scaled = (wide_part * input_gain[None, :]).astype(jnp.bfloat16)

    def add_product(weight):
        return jnp.dot(scaled, weight, preferred_element_type=jnp.float32)

    summed = tuple((add_product(weight) for weight in weight_list))
    q_acc, qrot_acc, latent_raw, rot_acc, value_acc, gate_acc, square_sum = summed + (
        jnp.sum(wide_part * wide_part, axis=1),
    )
    row_scale = lax.rsqrt(square_sum / D_MODEL + norm_eps)[:, None]
    positions = lax.axis_index("sp") * tok_rows + jnp.arange(tok_rows, dtype=jnp.int32)
    cos_table, sine_table = rotary_tables(positions, ROT_DIM // 2)
    latent = (
        latent_raw
        * lax.rsqrt(jnp.mean(latent_raw * latent_raw, axis=1, keepdims=True) + norm_eps)
        * kv_gain[None, :]
    ).astype(jnp.bfloat16)
    key_rot = rotate_half(rot_acc * row_scale, cos_table, sine_table).astype(jnp.bfloat16)
    gated_input = (value_acc * row_scale * jax.nn.sigmoid(gate_acc * row_scale)).astype(
        jnp.bfloat16
    )
    scale = LOG2E / math.sqrt(NOPE_DIM + ROT_DIM)
    q_rot = rotate_half(
        (qrot_acc * (row_scale * scale)).reshape(tok_rows, heads_here, ROT_DIM),
        cos_table[:, None, :],
        sine_table[:, None, :],
    ).reshape(tok_rows, heads_here * ROT_DIM)
    q_rot = jnp.concatenate([q_rot[: tok_rows // 2], q_rot[tok_rows // 2 :]], axis=1)
    packed = jnp.concatenate([q_acc * (row_scale * scale), q_rot], axis=0).astype(jnp.bfloat16)
    t = lax.axis_index("tp")
    mine = lax.dynamic_slice_in_dim(latent, t * 48, 48, 0)
    folds = key_rot.reshape(6, 4, 16, 32).transpose(0, 2, 1, 3).reshape(6, 16, 128)
    fold = lax.dynamic_index_in_dim(folds, jnp.minimum(t, 5), 0, keepdims=False)
    share = jnp.concatenate([mine[:, :128], mine[:, 128:], fold], axis=0)
    return layer(
        packed,
        share,
        gated_input,
        key_up,
        value_up,
        conv_taps,
        conv_ln_gain[None, :],
        conv_ln_bias[None, :],
        att_out_gain[None, :],
        conv_out_gain[None, :],
        att_out_weight,
        conv_out_weight,
    )


def solution(mesh):
    return jax.shard_map(
        shards,
        mesh=mesh,
        in_specs=(
            P("sp", "tp"),
            P(),
            P(None, "tp"),
            P(None, "tp"),
            P(),
            P(),
            P(),
            P(None, "tp"),
            P(None, "tp"),
            P(None, "tp"),
            P(None, "tp"),
            P(None, "tp"),
            P("tp"),
            P("tp"),
            P("tp"),
            P("tp"),
            P("tp", None),
            P("tp", None),
        ),
        out_specs=P("sp", "tp"),
        check_vma=False,
    )
```

time: 486 us -> 129 us (0.27)
  the two profiles are of different devices: /device:TPU:504 before, /device:TPU:11 now
where the time goes in v2:
time: 129 us
  Pallas kernels  89.3 us (69%)
  waiting for transfers between devices  19.5 us (15%)
  local copies, waits for them, and re-layouts  6.59 us (5%)
  starting transfers between devices  5.11 us (4%)
  other arithmetic  4.01 us (3%)
  matrix products  3.95 us (3%)
    pallas_call x1, Pallas kernels, layer(): pl.pallas_call(layer_kernel, out_shape=jax.ShapeDtypeStruct((ROWS, 256),...  89.3 us
    all_to_all x1, waiting for transfers between devices, copy_for_each(): lax.all_to_all(jnp.broadcast_to(x[None], (peers, *x.shape)), axis, 0, 0,...  19.5 us
    all_to_all x1, starting transfers between devices, copy_for_each(): lax.all_to_all(jnp.broadcast_to(x[None], (peers, *x.shape)), axis, 0, 0,...  5.11 us
    unnamed x20, local copies, waits for them, and re-layouts  4.32 us
    dot_general x6, matrix products, add_product(): return jnp.dot(scaled, weight, preferred_element_type=jnp.float32)  3.95 us
  transfers between devices with their start and end apart: 1, of which 1 were waited for; matrix products, arithmetic and copies ran while one was open for 0% of the time, Pallas kernels for 0%

profile of v2, /device:TPU:11, one launch (start us, length us, event | category | flops | bytes accessed | tf_op | source)
XLA Modules:
  0.0 128.7 jit_solution(17390239301246923027)
XLA Ops:
  0.0 0.0 copy-start
  0.0 1.2 copy.24
  1.2 1.3 %broadcast_in_dim.10 = bf16[8,384,256]{1,2,0:T(8,128)(2,1)} broadcast(bf16[384,256]{0,1:T(8,128)(2,1)S(1)} %copy.24), dimensions={1,2} | broadcast | bytes 1769472 | tf_op jit(solution)/shard_map/broadcast_in_dim | solution.py:26
  2.5 5.1 %all-to-all-start = ((bf16[8,384,256]{1,2,0:T(8,128)(2,1)}), bf16[8,384,256]{1,2,0:T(8,128)(2,1)S(1)}, u32[]{:S(2)}, u32[]{:S(2)}) async-start(bf16[8,384,256]{1,2,0:T(8,128)(2,1)} %broadcast_in_dim.10), calls=%async_computation | async-start | bytes 3145728 | tf_op jit(solution)/shard_map/all_to_all | solution.py:26
  7.6 0.0 copy-start.5
  7.6 19.5 %all-to-all-done = bf16[8,384,256]{1,2,0:T(8,128)(2,1)S(1)} async-done(((bf16[8,384,256]{1,2,0:T(8,128)(2,1)}), bf16[8,384,256]{1,2,0:T(8,128)(2,1)S(1)}, u32[]{:S(2)}, u32[]{:S(2)}) %all-to-all-start) | async-done | bytes 1572896 | tf_op jit(solution)/shard_map/all_to_all | solution.py:26
  27.1 0.0 copy-start.1
  27.1 0.4 multiply_reduce_fusion
  27.5 0.7 copy-done.1
  28.3 0.0 copy-done.5
  28.3 0.0 copy-start.3
  28.3 1.8 %fusion = bf16[384,2048]{0,1:T(8,128)(2,1)S(1)} fusion(f32[2048]{0:T(1024)S(1)} %copy-done.5, bf16[8,384,256]{1,2,0:T(8,128)(2,1)} %copy-done.1), kind=kLoop, calls=%fused_computation.1 | loop fusion | flops 2359296 | bytes 3153920 | tf_op jit(solution)/shard_map/convert_element_type | solution.py:558
  30.1 0.0 copy-start.4
  30.1 0.0 copy-done.3
  30.1 0.4 convolution_multiply_fusion.3
  30.5 0.0 copy-start.7
  30.5 0.5 copy-done.4
  31.0 0.3 convolution_multiply_fusion.4
  31.3 0.2 subtract_convert_fusion
  31.6 0.1 fusion.10
  31.6 0.1 copy.26
  31.8 0.1 copy.25
  31.9 0.0 copy-done.7
  31.9 0.6 fusion.6
  32.5 0.1 concatenate.27
  32.7 0.1 concatenate.26
  32.8 0.2 maximum_bitcast_fusion
  33.0 0.2 copy.27
  33.2 0.0 copy-start.6
  33.2 0.1 reshape.98
  33.3 0.0 copy-done
  33.3 0.0 copy-start.2
  33.3 0.7 multiply_reduce_fusion.1
  34.0 0.0 copy-start.8
  34.0 0.1 dynamic-slice
  34.1 0.0 copy-done.6
  34.1 0.1 fusion.9
  34.2 0.1 copy-done.2
  34.3 0.6 convolution_multiply_fusion.1
  35.0 0.1 copy-done.8
  35.1 1.3 fusion.7.gated_ref
  36.4 0.7 maximum_maximum_fusion.q_ref
  37.1 0.6 pad_maximum_fusion.share_ref
  37.7 89.3 %layer.1 = bf16[384,256]{1,0:T(8,128)(2,1)} custom-call(bf16[576,128]{1,0:T(8,128)(2,1)} %maximum_maximum_fusion.q_ref, bf16[112,128]{1,0:T(8,128)(2,1)} %pad_maximum_fusion.share_ref, bf16[384,128]{1,0:T(8,128)(2,1)} %fusion.7.gated_ref, bf16[256,128]{1,0:T(8,128)(2,1)} %key_up_ref.1, bf16[256,128]{1,0:T(8,128)(2,1)} %value_up_ref.1, f32[31,128]{1,0:T(8,128)} %taps_ref.1, ...), custom_call_target="tpu_custom_call" | custom-call | tf_op jit(solution)/shard_map/layer/pallas_call | solution.py:486
  127.1 1.6 %copy.29 = bf16[384,256]{1,0:T(8,128)(2,1)} copy(bf16[384,256]{1,0:T(8,128)(2,1)} %layer.1) | data formatting | bytes 393216
  (8 shorter events, 0.1 us)
Async XLA Ops:
  0.0 33.3 %copy-start = (bf16[2048,256]{1,0:T(8,128)(2,1)S(1)}, bf16[2048,256]{1,0:T(8,128)(2,1)}, u32[]{:S(2)}) copy-start(bf16[2048,256]{1,0:T(8,128)(2,1)} %param.22) | copy-start | bytes 3145732
  2.5 24.6 %all-to-all-start = ((bf16[8,384,256]{1,2,0:T(8,128)(2,1)}), bf16[8,384,256]{1,2,0:T(8,128)(2,1)S(1)}, u32[]{:S(2)}, u32[]{:S(2)}) async-start(bf16[8,384,256]{1,2,0:T(8,128)(2,1)} %broadcast_in_dim.10), calls=%async_computation | async-start | bytes 3145728 | tf_op jit(solution)/shard_map/all_to_all | solution.py:26
  7.6 20.7 %copy-start.5 = (f32[2048]{0:T(1024)S(1)}, f32[2048]{0:T(1024)}, u32[]{:S(2)}) copy-start(f32[2048]{0:T(1024)} %param.19) | copy-start | bytes 24580
  27.1 1.2 copy-start.1
  28.3 1.8 %copy-start.3 = (bf16[2048,64]{0,1:T(8,128)(2,1)S(1)}, bf16[2048,64]{0,1:T(8,128)(2,1)}, u32[]{:S(2)}) copy-start(bf16[2048,64]{0,1:T(8,128)(2,1)} %param.21) | copy-start | bytes 786436
  30.1 0.9 copy-start.4
  30.5 1.4 %copy-start.7 = (bf16[2048,128]{1,0:T(8,128)(2,1)S(1)}, bf16[2048,128]{1,0:T(8,128)(2,1)}, u32[]{:S(2)}) copy-start(bf16[2048,128]{1,0:T(8,128)(2,1)} %param.20) | copy-start | bytes 1572868
  33.2 1.0 copy-start.6
  33.3 1.0 copy-start.2
  34.0 1.1 copy-start.8

commit v3 on v2

--- a/solution.py
+++ b/solution.py
@@ -2,6 +2,7 @@
 
 import jax
 import jax.numpy as jnp
+import numpy as np
 from jax import lax
 from jax.experimental import pallas as pl
 from jax.experimental.pallas import tpu as pltpu
@@ -10,50 +11,12 @@
 D_MODEL = 2048
 NOPE_DIM = 64
 ROT_DIM = 32
-VALUE_DIM = 64
 CONV_CH = 1024
 KERNEL = 31
-ATT_WIDTH = 1024
-
 
 norm_eps = 1e-06
 far_below = -1e30
 rope_base = 10000.0
-
-
-def copy_for_each(x, axis):
-    peers = lax.axis_size(axis)
-    return lax.all_to_all(jnp.broadcast_to(x[None], (peers, *x.shape)), axis, 0, 0, tiled=True)
-
-
-def in_order(pieces, dim):
-    pieces = jnp.moveaxis(pieces, 0, dim)
-    shape = pieces.shape
-    return pieces.reshape(*shape[:dim], shape[dim] * shape[dim + 1], *shape[dim + 2 :])
-
-
-def gathered_copies(x, axis, dim):
-    pieces = copy_for_each(x, axis)
-    return in_order(pieces, dim)
-
-
-def rotary_tables(positions, half_dim):
-    frequency = rope_base ** (-jnp.arange(half_dim, dtype=jnp.float32) / half_dim)
-    angles = positions.astype(jnp.float32)[:, None] * frequency[None, :]
-    return (jnp.cos(angles), jnp.sin(angles))
-
-
-def rotate_half(values, cos_table, sine_table):
-    half_dim = cos_table.shape[-1]
-    front_half = values[..., :half_dim]
-    back_half = values[..., half_dim:]
-    return jnp.concatenate(
-        [
-            front_half * cos_table - back_half * sine_table,
-            back_half * cos_table + front_half * sine_table,
-        ],
-        axis=-1,
-    )
 
 
 MESH = pl.DeviceIdType.MESH
@@ -61,7 +24,7 @@
 SHARE = 112
 KSETS = 16
 PIECE = 4 * ROWS
-LOG2E = 1.4426950408889634
+SCALE = 1.4426950408889634 / math.sqrt(NOPE_DIM + ROT_DIM)
 
 
 def ring_peers(tp):
@@ -126,13 +89,17 @@
 
 
 def layer_kernel(
-    q_ref, share_ref, gated_ref, key_up_ref, value_up_ref, taps_ref, ln_gain_ref, ln_bias_ref,
-    att_gain_ref, conv_gain_ref, att_w_ref, conv_w_ref, out_ref,
+    tokens_hbm, query_hbm, query_rot_hbm, kv_down_hbm, rot_down_hbm, key_up_hbm, value_up_hbm,
+    conv_value_hbm, conv_gate_hbm, att_w_ref, conv_w_ref, near_cos_hbm, near_sin_hbm,
+    base_cos_ref, base_sin_ref, input_gain_ref, kv_gain_ref,
+    taps_ref, ln_gain_ref, ln_bias_ref, att_gain_ref, conv_gain_ref, out_ref,
+    tbuf, scaled, wall, wqr, wrd, wkvd, kup, vup, near_cos, near_sin, spun,
+    q_ref, share_ref, gated_ref,
     qraw, qbuf, kbuf, kk, vv, wkv, top, acc, o_send, l_send, o_recv, l_recv, own_out, own_lse,
     halo, padded, conv_out, mom_send, mom_recv, cbuf, abuf, weights, gains, gain_all, branch,
     q_ssem, q_rsem, k_ssem, k_rsem, f_ssem, f_rsem, ag_ssem, ag_rsem, o_ssem, o_rsem, l_ssem, l_rsem,
     h_ssem, h_rsem, m_ssem, m_rsem, c_ssem, c_rsem, a_ssem, a_rsem, w_ssem, w_rsem, g_ssem, g_rsem,
-    own_sem,
+    own_sem, t_ssem, t_rsem, load_sem,
 ):
     sp, tp = lax.axis_index("sp"), lax.axis_index("tp")
     z, y = sp // 8, sp % 8
@@ -150,6 +117,27 @@
     pair = z * 8 + (y + 1 - 2 * parity)
     after, before_sp = (sp + 1) % 64, (sp + 63) % 64
 
+    loads = [
+        pltpu.make_async_copy(src, dst, load_sem.at[n])
+        for n, (src, dst) in enumerate(
+            (
+                (tokens_hbm, tbuf.at[tp]),
+                (query_rot_hbm, wqr),
+                (rot_down_hbm, wrd),
+                (key_up_hbm, kup),
+                (value_up_hbm, vup),
+                (query_hbm, wall.at[:, pl.ds(0, 128)]),
+                (conv_value_hbm, wall.at[:, pl.ds(128, 128)]),
+                (conv_gate_hbm, wall.at[:, pl.ds(256, 128)]),
+                (kv_down_hbm, wkvd),
+                (near_cos_hbm, near_cos),
+                (near_sin_hbm, near_sin),
+            )
+        )
+    ]
+    for load in loads:
+        load.start()
+
     barrier = pltpu.get_barrier_semaphore()
     for i in range(1, 4):
         pl.semaphore_signal(
@@ -167,8 +155,78 @@
             src_ref=src, dst_ref=dst, send_sem=ssem, recv_sem=rsem, device_id=to, device_id_type=MESH
         )
 
-    halo_copy = remote(gated_ref.at[pl.ds(ROWS - 32, 32)], halo, h_ssem, h_rsem, (after, tp))
-    halo_copy.start()
+    tokens_gather = RingGather(tbuf, 0, ROWS, ROWS // 2, t_ssem, t_rsem, sp, tp)
+    loads[0].wait()
+    tokens_gather.begin()
+
+    gains[...] = jnp.zeros(gains.shape, f32)
+    gains[0:1, :] = att_gain_ref[...]
+    gains[1:2, :] = conv_gain_ref[...]
+    loads[1].wait()
+    loads[2].wait()
+    wall[:, pl.ds(384, 128)] = jnp.concatenate(
+        [wqr[...].astype(f32), wrd[...].astype(f32), jnp.zeros((D_MODEL, 32), f32)], axis=1
+    ).astype(bf)
+    loads[3].wait()
+    loads[4].wait()
+    lane = lax.broadcasted_iota(jnp.int32, (256, 128), 1)
+    for n, ref in enumerate((kup, vup)):
+        w = ref[...].astype(f32)
+        wkv[:, pl.ds(256 * n, 128)] = jnp.where(lane < 64, w, 0.0).astype(bf)
+        wkv[:, pl.ds(256 * n + 128, 128)] = jnp.where(lane < 64, pltpu.roll(w, 64, 1), 0.0).astype(bf)
+
+    def scale_block(t):
+        columns = pl.ds(pl.multiple_of(256 * t, 256), 256)
+        x = tbuf[t].astype(f32)
+        scaled[:, columns] = (x * input_gain_ref[:, columns]).astype(bf)
+        return x * x
+
+    squares = scale_block(tp)
+    tokens_gather.relay()
+    squares = squares + scale_block(tokens_gather.left)
+    squares = squares + scale_block(tokens_gather.right)
+    tokens_gather.relay_far()
+    tokens_gather.finish()
+    squares = squares + scale_block(tokens_gather.far)
+    for t in (tp, tokens_gather.left, tokens_gather.right, tokens_gather.far):
+        squares = squares + scale_block(t + 1 - 2 * (t % 2))
+    row_scale = lax.rsqrt(jnp.sum(squares, axis=1, keepdims=True) / D_MODEL + norm_eps)
+
+    for load in loads[5:]:
+        load.wait()
+    raw = jnp.dot(
+        scaled[pl.ds(pl.multiple_of(48 * tp, 16), 48), :], wkvd[...], preferred_element_type=f32
+    )
+    power = jnp.sum(raw * raw, axis=1, keepdims=True) / 256
+    latent = (raw * lax.rsqrt(power + norm_eps) * kv_gain_ref[...]).astype(bf)
+    share_ref[0:48, :] = latent[:, 0:128]
+    share_ref[48:96, :] = latent[:, 128:256]
+
+    tag = lax.broadcasted_iota(jnp.int32, (ROWS, 128), 1)
+    low = tag < 64
+    sums = jnp.dot(scaled[...], wall[...], preferred_element_type=f32)
+    flat = sums[:, 384:512] * row_scale
+    cos_base, sin_base = base_cos_ref[pl.ds(sp, 1), :], base_sin_ref[pl.ds(sp, 1), :]
+    cosine = near_cos[...] * cos_base - near_sin[...] * sin_base
+    sine = near_sin[...] * cos_base + near_cos[...] * sin_base
+    forward_half = tag % 32 < 16
+    other = jnp.where(forward_half, pltpu.roll(flat, 112, 1), pltpu.roll(flat, 16, 1))
+    turned_rows = flat * cosine + other * jnp.where(forward_half, -sine, sine)
+    spun[...] = turned_rows
+    short = lax.broadcasted_iota(jnp.int32, (16, 128), 1) // 32
+    fold = jnp.zeros((16, 128), f32)
+    first_row = 64 * jnp.minimum(tp, 5)
+    for j in range(4):
+        part = spun[pl.ds(pl.multiple_of(first_row + 16 * j, 16), 16), :]
+        fold = jnp.where(short == j, pltpu.roll(part, (64 + 32 * j) % 128, 1), fold)
+    share_ref[96:112, :] = fold.astype(bf)
+    q_ref[0:ROWS, :] = (sums[:, 0:128] * (row_scale * SCALE)).astype(bf)
+    half = ROWS // 2
+    q_ref[ROWS : ROWS + half, :] = (
+        jnp.where(low[0:half], turned_rows[0:half], pltpu.roll(turned_rows[half:ROWS], 64, 1)) * SCALE
+    ).astype(bf)
+    gated = (sums[:, 128:256] * row_scale * jax.nn.sigmoid(sums[:, 256:384] * row_scale)).astype(bf)
+    gated_ref[...] = gated
 
     slot = 4 * mine + 2 * parity + z % 2
 
@@ -181,6 +239,9 @@
     for i in range(1, 8):
         key_copy(i).start()
 
+    halo_copy = remote(gated_ref.at[pl.ds(ROWS - 32, 32)], halo, h_ssem, h_rsem, (after, tp))
+    halo_copy.start()
+
     def query_copy(i):
         return remote(
             q_ref, qraw.at[i - 1], q_ssem.at[i - 1], q_rsem.at[i - 1], (member_sp((mine + i) % 4), tp)
@@ -188,18 +249,6 @@
 
     for i in range(1, 4):
         query_copy(i).start()
-
-    gains[...] = jnp.zeros(gains.shape, f32)
-    gains[0:1, :] = att_gain_ref[...]
-    gains[1:2, :] = conv_gain_ref[...]
-    lane = lax.broadcasted_iota(jnp.int32, (256, 128), 1)
-    for n, ref in enumerate((key_up_ref, value_up_ref)):
-        w = ref[...].astype(f32)
-        wkv[:, pl.ds(256 * n, 128)] = jnp.where(lane < 64, w, 0.0).astype(bf)
-        wkv[:, pl.ds(256 * n + 128, 128)] = jnp.where(lane < 64, pltpu.roll(w, 64, 1), 0.0).astype(bf)
-
-    tag = lax.broadcasted_iota(jnp.int32, (ROWS, 128), 1)
-    low = tag < 64
 
     def unpack(ref, member):
         nope = ref[0:ROWS, :].astype(f32)
@@ -461,6 +510,7 @@
     att_gather.finish()
     out_ref[...] = (branch[...] + product(abuf, 0)).astype(bf)
 
+    tokens_gather.drain()
     halo_copy.wait_send()
     for i in range(1, 8):
         key_copy(i).wait_send()
@@ -486,9 +536,23 @@
     return pl.pallas_call(
         layer_kernel,
         out_shape=jax.ShapeDtypeStruct((ROWS, 256), bf),
-        in_specs=[vmem] * 10 + [anywhere] * 2,
+        in_specs=[anywhere] * 13 + [vmem] * 9,
         out_specs=vmem,
         scratch_shapes=[
+            pltpu.VMEM((8, ROWS, 256), bf),
+            pltpu.VMEM((ROWS, D_MODEL), bf),
+            pltpu.VMEM((D_MODEL, 512), bf),
+            pltpu.VMEM((D_MODEL, 64), bf),
+            pltpu.VMEM((D_MODEL, 32), bf),
+            pltpu.VMEM((D_MODEL, 256), bf),
+            pltpu.VMEM((256, 128), bf),
+            pltpu.VMEM((256, 128), bf),
+            pltpu.VMEM((ROWS, 128), f32),
+            pltpu.VMEM((ROWS, 128), f32),
+            pltpu.VMEM((ROWS, 128), f32),
+            pltpu.VMEM((ROWS + ROWS // 2, 128), bf),
+            pltpu.VMEM((SHARE, 128), bf),
+            pltpu.VMEM((ROWS, 128), bf),
             pltpu.VMEM((3, ROWS + ROWS // 2, 128), bf),
             pltpu.VMEM((4, 2, ROWS, 128), bf),
             pltpu.VMEM((8, KSETS, SHARE, 128), bf),
@@ -517,11 +581,19 @@
             dma((3,)), dma((3,)), dma((8,)), dma((4,)), dma((4,)), dma((4,)), dma((4, 9)), dma((4, 9)),
             dma((4,)), dma((4,)), dma((4,)), dma((4,)), dma, dma, dma((8,)), dma((8,)),
             dma((9,)), dma((9,)), dma((9,)), dma((9,)), dma((2, 8)), dma((2, 8)), dma((8,)), dma((8,)),
-            dma((2,)),
+            dma((2,)), dma((9,)), dma((9,)), dma((11,)),
         ],
         compiler_params=pltpu.CompilerParams(collective_id=1, has_side_effects=True),
         name="layer",
     )(*args)
+
+
+def rotary_tables():
+    lanes = np.arange(128)
+    frequency = rope_base ** (-(lanes % 16) / 16.0)
+    near = np.arange(ROWS)[:, None] * frequency[None, :]
+    base = (np.arange(64) * ROWS)[:, None] * frequency[None, :]
+    return tuple(np.asarray(f(a), np.float32) for a in (near, base) for f in (np.cos, np.sin))
 
 
 def shards(
@@ -544,64 +616,30 @@
     att_out_weight,
     conv_out_weight,
 ):
-    tok_rows = tokens.shape[0]
-    heads_here = key_up.shape[1] // NOPE_DIM
-    weight_list = (
+    near_cos, near_sin, base_cos, base_sin = rotary_tables()
+    return layer(
+        tokens,
         query_weight,
         query_rot_weight,
         kv_down,
         rot_down,
+        key_up,
+        value_up,
         conv_value_weight,
         conv_gate_weight,
-    )
-    wide_part = gathered_copies(tokens, "tp", 1).astype(jnp.float32)
-    scaled = (wide_part * input_gain[None, :]).astype(jnp.bfloat16)
-
-    def add_product(weight):
-        return jnp.dot(scaled, weight, preferred_element_type=jnp.float32)
-
-    summed = tuple((add_product(weight) for weight in weight_list))
-    q_acc, qrot_acc, latent_raw, rot_acc, value_acc, gate_acc, square_sum = summed + (
-        jnp.sum(wide_part * wide_part, axis=1),
-    )
-    row_scale = lax.rsqrt(square_sum / D_MODEL + norm_eps)[:, None]
-    positions = lax.axis_index("sp") * tok_rows + jnp.arange(tok_rows, dtype=jnp.int32)
-    cos_table, sine_table = rotary_tables(positions, ROT_DIM // 2)
-    latent = (
-        latent_raw
-        * lax.rsqrt(jnp.mean(latent_raw * latent_raw, axis=1, keepdims=True) + norm_eps)
-        * kv_gain[None, :]
-    ).astype(jnp.bfloat16)
-    key_rot = rotate_half(rot_acc * row_scale, cos_table, sine_table).astype(jnp.bfloat16)
-    gated_input = (value_acc * row_scale * jax.nn.sigmoid(gate_acc * row_scale)).astype(
-        jnp.bfloat16
-    )
-    scale = LOG2E / math.sqrt(NOPE_DIM + ROT_DIM)
-    q_rot = rotate_half(
-        (qrot_acc * (row_scale * scale)).reshape(tok_rows, heads_here, ROT_DIM),
-        cos_table[:, None, :],
-        sine_table[:, None, :],
-    ).reshape(tok_rows, heads_here * ROT_DIM)
-    q_rot = jnp.concatenate([q_rot[: tok_rows // 2], q_rot[tok_rows // 2 :]], axis=1)
-    packed = jnp.concatenate([q_acc * (row_scale * scale), q_rot], axis=0).astype(jnp.bfloat16)
-    t = lax.axis_index("tp")
-    mine = lax.dynamic_slice_in_dim(latent, t * 48, 48, 0)
-    folds = key_rot.reshape(6, 4, 16, 32).transpose(0, 2, 1, 3).reshape(6, 16, 128)
-    fold = lax.dynamic_index_in_dim(folds, jnp.minimum(t, 5), 0, keepdims=False)
-    share = jnp.concatenate([mine[:, :128], mine[:, 128:], fold], axis=0)
-    return layer(
-        packed,
-        share,
-        gated_input,
-        key_up,
-        value_up,
+        att_out_weight,
+        conv_out_weight,
+        jnp.asarray(near_cos),
+        jnp.asarray(near_sin),
+        jnp.asarray(base_cos),
+        jnp.asarray(base_sin),
+        input_gain[None, :],
+        kv_gain[None, :],
         conv_taps,
         conv_ln_gain[None, :],
         conv_ln_bias[None, :],
         att_out_gain[None, :],
         conv_out_gain[None, :],
-        att_out_weight,
-        conv_out_weight,
     )
 
 

time: 129 us -> 111 us (0.86)
  the two profiles are of different devices: /device:TPU:11 before, /device:TPU:467 now
where the time goes in v3:
time: 111 us; the launch traced here: 110 us
  Pallas kernels  106 us (95%)
  local copies, waits for them, and re-layouts  4.62 us (4%)
    pallas_call x1, Pallas kernels, layer(): pl.pallas_call(layer_kernel, out_shape=jax.ShapeDtypeStruct((ROWS, 256),...  106 us
    unnamed x5, local copies, waits for them, and re-layouts  4.62 us

profile of v3, /device:TPU:467, one launch (start us, length us, event | category | flops | bytes accessed | tf_op | source)
XLA Modules:
  0.0 110.3 jit_solution(12022854954003976940)
XLA Ops:
  0.0 0.0 copy-start
  0.0 2.0 %copy.23.query_rot_hbm = bf16[2048,64]{1,0:T(8,128)(2,1)} copy(bf16[2048,64]{0,1:T(8,128)(2,1)} %param.25) | data formatting | bytes 524288 | tf_op args[3]
  2.0 0.0 copy-done
  2.0 1.0 copy.24.rot_down_hbm
  3.0 105.7 %layer.1 = bf16[384,256]{1,0:T(8,128)(2,1)} custom-call(bf16[384,256]{1,0:T(8,128)(2,1)} %tokens_hbm.1, bf16[2048,128]{1,0:T(8,128)(2,1)} %query_hbm.1, bf16[2048,64]{1,0:T(8,128)(2,1)} %copy.23.query_rot_hbm, bf16[2048,256]{1,0:T(8,128)(2,1)} %kv_down_hbm.1, bf16[2048,32]{1,0:T(8,128)(2,1)} %copy.24.rot_down_hbm, bf16[256,128]{1,0:T(8,128)(2,1)} %key_up_hbm.1, ...), custom_call_target="tpu_custom_call" | custom-call | tf_op jit(solution)/shard_map/layer/pallas_call | solution.py:536
  108.7 1.6 %copy.26 = bf16[384,256]{1,0:T(8,128)(2,1)} copy(bf16[384,256]{1,0:T(8,128)(2,1)} %layer.1) | data formatting | bytes 393216
Async XLA Ops:
  0.0 2.0 %copy-start = (bf16[2048,32]{0,1:T(8,128)(2,1)S(1)}, bf16[2048,32]{0,1:T(8,128)(2,1)}, u32[]{:S(2)}) copy-start(bf16[2048,32]{0,1:T(8,128)(2,1)} %param.27) | copy-start | bytes 393220

commit v4 on v3

--- a/solution.py
+++ b/solution.py
@@ -37,14 +37,15 @@
 
 
 class RingGather:
-    def __init__(self, buf, lo, hi, mid, send, recv, sp, tp):
-        self.buf, self.lo, self.hi, self.mid = buf, lo, hi, mid
+    def __init__(self, buf, lo, size, send, recv, sp, tp):
+        self.buf, self.lo, self.size = buf, lo, size
         self.send, self.recv, self.sp, self.tp = send, recv, sp, tp
         self.right, self.left, self.far, self.partner = ring_peers(tp)
 
     def piece(self, slot, part=None):
-        lo, hi = {None: (self.lo, self.hi), 0: (self.lo, self.mid), 1: (self.mid, self.hi)}[part]
-        return self.buf.at[slot, pl.ds(lo, hi - lo)]
+        size = self.size if part is None else self.size // 2
+        start = self.lo + size if part == 1 else self.lo
+        return self.buf.at[slot, pl.ds(start, size)]
 
     def copy(self, slot, part, sem, to):
         return pltpu.make_async_remote_copy(
@@ -93,13 +94,13 @@
     conv_value_hbm, conv_gate_hbm, att_w_ref, conv_w_ref, near_cos_hbm, near_sin_hbm,
     base_cos_ref, base_sin_ref, input_gain_ref, kv_gain_ref,
     taps_ref, ln_gain_ref, ln_bias_ref, att_gain_ref, conv_gain_ref, out_ref,
-    tbuf, scaled, wall, wqr, wrd, wkvd, kup, vup, near_cos, near_sin, spun,
+    tbuf, scaled, wall, wqr, wrd, wkvd, kup, vup, near_cos, near_sin, p_send, p_recv,
     q_ref, share_ref, gated_ref,
     qraw, qbuf, kbuf, kk, vv, wkv, top, acc, o_send, l_send, o_recv, l_recv, own_out, own_lse,
     halo, padded, conv_out, mom_send, mom_recv, cbuf, abuf, weights, gains, gain_all, branch,
     q_ssem, q_rsem, k_ssem, k_rsem, f_ssem, f_rsem, ag_ssem, ag_rsem, o_ssem, o_rsem, l_ssem, l_rsem,
     h_ssem, h_rsem, m_ssem, m_rsem, c_ssem, c_rsem, a_ssem, a_rsem, w_ssem, w_rsem, g_ssem, g_rsem,
-    own_sem, t_ssem, t_rsem, load_sem,
+    own_sem, t_ssem, t_rsem, load_sem, p_ssem, p_rsem,
 ):
     sp, tp = lax.axis_index("sp"), lax.axis_index("tp")
     z, y = sp // 8, sp % 8
@@ -110,26 +111,32 @@
     def member_sp(member):
         return member_z(member, kind) * 8 + y
 
-    key_peers = []
-    for dz in range(8):
-        zz = (z + dz) % 8
-        key_peers.append(zz * 8 + 2 * ((residue + 4 - zz // 2) % 4) + parity)
-    pair = z * 8 + (y + 1 - 2 * parity)
+    place = 2 * parity + z % 2
+    z_other, y_other = z + 1 - 2 * (z % 2), y + 1 - 2 * parity
+    quad = (z_other * 8 + y, z * 8 + y_other, z_other * 8 + y_other)
+    orders = (0, 1, 3, 2)
+    pieces = [(mine + d) % 4 for d in orders]
+    far_quads = [None]
+    for j in range(1, 4):
+        m = (mine + 4 - orders[j]) % 4
+        far_quads.append((2 * m + z % 2) * 8 + 2 * ((residue + 4 - m) % 4) + parity)
     after, before_sp = (sp + 1) % 64, (sp + 63) % 64
 
+    own_rows = pl.ds(pl.multiple_of(256 * tp, 256), 256)
+    wrd[32:128, :] = jnp.zeros((96, 256), bf)
     loads = [
         pltpu.make_async_copy(src, dst, load_sem.at[n])
         for n, (src, dst) in enumerate(
             (
                 (tokens_hbm, tbuf.at[tp]),
-                (query_rot_hbm, wqr),
-                (rot_down_hbm, wrd),
+                (kv_down_hbm.at[own_rows], wkvd),
+                (rot_down_hbm.at[:, own_rows], wrd.at[pl.ds(0, 32)]),
                 (key_up_hbm, kup),
                 (value_up_hbm, vup),
                 (query_hbm, wall.at[:, pl.ds(0, 128)]),
                 (conv_value_hbm, wall.at[:, pl.ds(128, 128)]),
                 (conv_gate_hbm, wall.at[:, pl.ds(256, 128)]),
-                (kv_down_hbm, wkvd),
+                (query_rot_hbm, wqr),
                 (near_cos_hbm, near_cos),
                 (near_sin_hbm, near_sin),
             )
@@ -143,83 +150,147 @@
         pl.semaphore_signal(
             barrier, inc=1, device_id=(member_sp((mine + i) % 4), tp), device_id_type=MESH
         )
+        pl.semaphore_signal(barrier, inc=1, device_id=(far_quads[i], tp), device_id_type=MESH)
+        pl.semaphore_signal(barrier, inc=1, device_id=(quad[i - 1], tp), device_id_type=MESH)
     for i in range(1, 8):
-        pl.semaphore_signal(barrier, inc=1, device_id=(key_peers[i], tp), device_id_type=MESH)
         pl.semaphore_signal(barrier, inc=1, device_id=(sp, (tp + i) % 8), device_id_type=MESH)
-    pl.semaphore_signal(barrier, inc=1, device_id=(pair, tp), device_id_type=MESH)
     pl.semaphore_signal(barrier, inc=1, device_id=(before_sp, tp), device_id_type=MESH)
-    pl.semaphore_wait(barrier, 19)
+    pl.semaphore_wait(barrier, 17)
 
     def remote(src, dst, ssem, rsem, to):
         return pltpu.make_async_remote_copy(
             src_ref=src, dst_ref=dst, send_sem=ssem, recv_sem=rsem, device_id=to, device_id_type=MESH
         )
 
-    tokens_gather = RingGather(tbuf, 0, ROWS, ROWS // 2, t_ssem, t_rsem, sp, tp)
-    loads[0].wait()
+    def scale_block(t):
+        columns = pl.ds(pl.multiple_of(256 * t, 256), 256)
+        x = tbuf[t].astype(f32)
+        scaled[:, columns] = (x * input_gain_ref[:, columns]).astype(bf)
+        return x * x
+
+    tag = lax.broadcasted_iota(jnp.int32, (ROWS, 128), 1)
+    low = tag < 64
+    tokens_gather = RingGather(tbuf, 0, ROWS, t_ssem, t_rsem, sp, tp)
+    for load in loads[0:3]:
+        load.wait()
+    squares = scale_block(tp)
+    mine_scaled = scaled[:, own_rows]
+    p_send[:, 0:256] = jnp.dot(mine_scaled, wkvd[...], preferred_element_type=f32).astype(bf)
+    rot_part = lax.dot_general(
+        mine_scaled, wrd[...], (((1,), (1,)), ((), ())), preferred_element_type=f32
+    )
+    p_send[:, 256:384] = jnp.where(
+        tag == 32, jnp.sum(squares, axis=1, keepdims=True), rot_part
+    ).astype(bf)
+
+    def part_copy(j):
+        peer = (tp + j) % 8
+        return remote(
+            p_send.at[pl.ds(pl.multiple_of(48 * peer, 16), 48)],
+            p_recv.at[tp],
+            p_ssem.at[j],
+            p_rsem.at[tp],
+            (sp, peer),
+        )
+
+    for j in range(1, 8):
+        part_copy(j).start()
     tokens_gather.begin()
 
     gains[...] = jnp.zeros(gains.shape, f32)
     gains[0:1, :] = att_gain_ref[...]
     gains[1:2, :] = conv_gain_ref[...]
-    loads[1].wait()
-    loads[2].wait()
-    wall[:, pl.ds(384, 128)] = jnp.concatenate(
-        [wqr[...].astype(f32), wrd[...].astype(f32), jnp.zeros((D_MODEL, 32), f32)], axis=1
-    ).astype(bf)
-    loads[3].wait()
-    loads[4].wait()
+    for load in loads[3:]:
+        load.wait()
     lane = lax.broadcasted_iota(jnp.int32, (256, 128), 1)
     for n, ref in enumerate((kup, vup)):
         w = ref[...].astype(f32)
         wkv[:, pl.ds(256 * n, 128)] = jnp.where(lane < 64, w, 0.0).astype(bf)
         wkv[:, pl.ds(256 * n + 128, 128)] = jnp.where(lane < 64, pltpu.roll(w, 64, 1), 0.0).astype(bf)
-
-    def scale_block(t):
-        columns = pl.ds(pl.multiple_of(256 * t, 256), 256)
-        x = tbuf[t].astype(f32)
-        scaled[:, columns] = (x * input_gain_ref[:, columns]).astype(bf)
-        return x * x
-
-    squares = scale_block(tp)
+    cos_base, sin_base = base_cos_ref[pl.ds(sp, 1), :], base_sin_ref[pl.ds(sp, 1), :]
+
+    def turn(rows, near_c, near_s):
+        cosine = near_c * cos_base - near_s * sin_base
+        sine = near_s * cos_base + near_c * sin_base
+        front = lax.broadcasted_iota(jnp.int32, rows.shape, 1) % 32 < 16
+        other = jnp.where(front, pltpu.roll(rows, 112, 1), pltpu.roll(rows, 16, 1))
+        return rows * cosine + other * jnp.where(front, -sine, sine)
+
+    share_rows = pl.ds(pl.multiple_of(48 * tp, 16), 48)
+    raw = p_send[share_rows, :].astype(f32)
+    for j in range(1, 8):
+        source = (tp + j) % 8
+        remote(
+            p_send.at[share_rows], p_recv.at[source], p_ssem.at[j], p_rsem.at[source], (sp, source)
+        ).wait_recv()
+        raw = raw + p_recv[source].astype(f32)
+    power = jnp.sum(raw[:, 0:256] * raw[:, 0:256], axis=1, keepdims=True) / 256
+    latent = (raw[:, 0:256] * lax.rsqrt(power + norm_eps) * kv_gain_ref[...]).astype(bf)
+    share_ref[0:48, :] = latent[:, 0:128]
+    share_ref[48:96, :] = latent[:, 128:256]
+    key_rows = raw[:, 256:384]
+    key_rows = key_rows * lax.rsqrt(key_rows[:, 32:33] / D_MODEL + norm_eps)
+    key_rows = turn(key_rows, near_cos[share_rows, :], near_sin[share_rows, :])
+    group = lax.broadcasted_iota(jnp.int32, (16, 128), 1) // 32
+    fold = jnp.zeros((16, 128), f32)
+    for j in range(3):
+        fold = jnp.where(group == j, pltpu.roll(key_rows[16 * j : 16 * j + 16], 32 * j, 1), fold)
+    share_ref[96:112, :] = fold.astype(bf)
+
+    def block(j):
+        return kbuf.at[tp, 4 * pieces[j] + place]
+
+    own_block = pltpu.make_async_copy(share_ref, block(0), own_sem.at[2])
+    own_block.start()
+
+    def key_copy(j):
+        return remote(share_ref, block(0), k_ssem.at[j], k_rsem.at[j], (far_quads[j], tp))
+
+    def quad_copy(j, n):
+        source = share_ref if j == 0 else block(j)
+        return remote(source, block(j), f_ssem.at[j, n], f_rsem.at[j, n], (quad[n], tp))
+
+    def spread(j):
+        if j > 0:
+            remote(share_ref, block(j), k_ssem.at[j], k_rsem.at[j], (far_quads[j], tp)).wait_recv()
+        for n in range(3):
+            quad_copy(j, n).start()
+
+    gathers = [
+        RingGather(kbuf, 4 * p, 4, ag_ssem.at[j], ag_rsem.at[j], sp, tp)
+        for j, p in enumerate(pieces)
+    ]
+    conv_gather = RingGather(cbuf, 0, ROWS, c_ssem, c_rsem, sp, tp)
+    att_gather = RingGather(abuf, 0, ROWS, a_ssem, a_rsem, sp, tp)
+
+    def begin(j):
+        for n in range(3):
+            quad_copy(j, n).wait_recv()
+        gathers[j].begin()
+
+    spread(0)
+    for j in range(1, 4):
+        key_copy(j).start()
+    own_block.wait()
+
     tokens_gather.relay()
     squares = squares + scale_block(tokens_gather.left)
     squares = squares + scale_block(tokens_gather.right)
+    begin(0)
     tokens_gather.relay_far()
+    spread(1)
+    spread(2)
     tokens_gather.finish()
     squares = squares + scale_block(tokens_gather.far)
     for t in (tp, tokens_gather.left, tokens_gather.right, tokens_gather.far):
         squares = squares + scale_block(t + 1 - 2 * (t % 2))
     row_scale = lax.rsqrt(jnp.sum(squares, axis=1, keepdims=True) / D_MODEL + norm_eps)
-
-    for load in loads[5:]:
-        load.wait()
-    raw = jnp.dot(
-        scaled[pl.ds(pl.multiple_of(48 * tp, 16), 48), :], wkvd[...], preferred_element_type=f32
+    flat = lax.dot_general(
+        scaled[...], wqr[...], (((1,), (1,)), ((), ())), preferred_element_type=f32
     )
-    power = jnp.sum(raw * raw, axis=1, keepdims=True) / 256
-    latent = (raw * lax.rsqrt(power + norm_eps) * kv_gain_ref[...]).astype(bf)
-    share_ref[0:48, :] = latent[:, 0:128]
-    share_ref[48:96, :] = latent[:, 128:256]
-
-    tag = lax.broadcasted_iota(jnp.int32, (ROWS, 128), 1)
-    low = tag < 64
+    flat = jnp.concatenate([flat * row_scale, jnp.zeros((ROWS, 64), f32)], axis=1)
+    turned_rows = turn(flat, near_cos[...], near_sin[...])
     sums = jnp.dot(scaled[...], wall[...], preferred_element_type=f32)
-    flat = sums[:, 384:512] * row_scale
-    cos_base, sin_base = base_cos_ref[pl.ds(sp, 1), :], base_sin_ref[pl.ds(sp, 1), :]
-    cosine = near_cos[...] * cos_base - near_sin[...] * sin_base
-    sine = near_sin[...] * cos_base + near_cos[...] * sin_base
-    forward_half = tag % 32 < 16
-    other = jnp.where(forward_half, pltpu.roll(flat, 112, 1), pltpu.roll(flat, 16, 1))
-    turned_rows = flat * cosine + other * jnp.where(forward_half, -sine, sine)
-    spun[...] = turned_rows
-    short = lax.broadcasted_iota(jnp.int32, (16, 128), 1) // 32
-    fold = jnp.zeros((16, 128), f32)
-    first_row = 64 * jnp.minimum(tp, 5)
-    for j in range(4):
-        part = spun[pl.ds(pl.multiple_of(first_row + 16 * j, 16), 16), :]
-        fold = jnp.where(short == j, pltpu.roll(part, (64 + 32 * j) % 128, 1), fold)
-    share_ref[96:112, :] = fold.astype(bf)
     q_ref[0:ROWS, :] = (sums[:, 0:128] * (row_scale * SCALE)).astype(bf)
     half = ROWS // 2
     q_ref[ROWS : ROWS + half, :] = (
@@ -227,17 +298,6 @@
     ).astype(bf)
     gated = (sums[:, 128:256] * row_scale * jax.nn.sigmoid(sums[:, 256:384] * row_scale)).astype(bf)
     gated_ref[...] = gated
-
-    slot = 4 * mine + 2 * parity + z % 2
-
-    def key_copy(i):
-        return remote(
-            share_ref, kbuf.at[tp, slot], k_ssem.at[i], k_rsem.at[mine], (key_peers[i], tp)
-        )
-
-    pltpu.make_async_copy(share_ref, kbuf.at[tp, slot], k_rsem.at[mine]).start()
-    for i in range(1, 8):
-        key_copy(i).start()
 
     halo_copy = remote(gated_ref.at[pl.ds(ROWS - 32, 32)], halo, h_ssem, h_rsem, (after, tp))
     halo_copy.start()
@@ -260,7 +320,13 @@
             rotary = jnp.concatenate([upper, lower], axis=0)
             qbuf[member, h] = jnp.where(low, body, jnp.where(tag < 96, rotary, 0.0)).astype(bf)
 
+    begin(1)
+    gathers[0].relay()
+    spread(3)
     unpack(q_ref, mine)
+    begin(2)
+    gathers[1].relay()
+    gathers[0].relay_far()
 
     halo_copy.wait_recv()
     edge = halo[...].astype(f32)
@@ -274,14 +340,9 @@
     sum_two = jnp.sum(total * total, axis=1, keepdims=True)
     mom_send[...] = jnp.transpose(jnp.where(tag == 0, sum_one, sum_two))[0:8, :]
 
-    def forward(p):
-        piece = kbuf.at[tp, pl.ds(4 * p + 2 * parity, 2)]
-        return remote(piece, piece, f_ssem.at[p], f_rsem.at[p], (pair, tp))
-
-    for p in range(4):
-        piece = kbuf.at[tp, pl.ds(4 * p + 2 * parity, 2)]
-        pltpu.make_async_copy(piece, piece, k_rsem.at[p]).wait()
-        forward(p).start()
+    begin(3)
+    gathers[2].relay()
+    gathers[1].relay_far()
 
     def moment_copy(j):
         return remote(
@@ -291,19 +352,9 @@
     for j in range(1, 8):
         moment_copy(j).start()
 
-    gathers = [
-        RingGather(kbuf, 4 * p, 4 * p + 4, 4 * p + 2, ag_ssem.at[p], ag_rsem.at[p], sp, tp)
-        for p in range(4)
-    ]
-    conv_gather = RingGather(cbuf, 0, ROWS, ROWS // 2, c_ssem, c_rsem, sp, tp)
-    att_gather = RingGather(abuf, 0, ROWS, ROWS // 2, a_ssem, a_rsem, sp, tp)
-
-    def begin(p):
-        forward(p).wait_recv()
-        gathers[p].begin()
-
     def assemble(p):
         slots = [4 * p + u for u in range(4)]
+        at = pl.ds(pl.multiple_of(p * PIECE, PIECE), PIECE)
         first = jnp.concatenate([kbuf[:, s, 0:48, :].reshape(ROWS, 128) for s in slots], axis=0)
         second = jnp.concatenate([kbuf[:, s, 48:96, :].reshape(ROWS, 128) for s in slots], axis=0)
         product = jnp.dot(
@@ -311,18 +362,18 @@
         )
         pieces = []
         for s in slots:
-            folded = kbuf[0:6, s, 96:112, :].astype(f32).reshape(96, 128)
+            folded = kbuf[:, s, 96:112, :].astype(f32).reshape(128, 128)
             turned = [
-                pltpu.roll(folded, (64 - 32 * j) % 128, 1).reshape(6, 1, 16, 128) for j in range(4)
+                pltpu.roll(folded, (64 - 32 * j) % 128, 1).reshape(8, 1, 16, 128) for j in range(3)
             ]
             pieces.append(jnp.concatenate(turned, axis=1).reshape(ROWS, 128))
         rotary = jnp.concatenate(pieces, axis=0)
         front = lax.broadcasted_iota(jnp.int32, (PIECE, 128), 1) < 64
         for h in range(2):
-            kk[h, pl.ds(p * PIECE, PIECE), :] = jnp.where(
+            kk[h, at, :] = jnp.where(
                 front, product[:, 128 * h : 128 * h + 128], rotary
             ).astype(bf)
-            vv[h, pl.ds(p * PIECE, PIECE), :] = jnp.where(
+            vv[h, at, :] = jnp.where(
                 front, product[:, 256 + 128 * h : 384 + 128 * h], 1.0
             ).astype(bf)
 
@@ -406,16 +457,11 @@
         pltpu.make_async_copy(conv_w_ref.at[:, own_columns], weights.at[1, tp], own_sem.at[1]),
     )
 
-    begin(0)
-    gathers[0].relay()
-    begin(1)
-    gathers[0].relay_far()
+    gathers[3].relay()
+    gathers[2].relay_far()
     gathers[0].finish()
-    assemble(0)
-    gathers[1].relay()
-    begin(2)
-    step(mine, 0, True)
-    gathers[1].relay_far()
+    assemble(pieces[0])
+    gathers[3].relay_far()
 
     mom_recv[tp] = mom_send[...]
     for j in range(1, 8):
@@ -431,42 +477,36 @@
     swished = jax.nn.silu(normed * ln_gain_ref[...] + ln_bias_ref[...])
     cbuf[tp] = swished.astype(bf)
 
+    conv_gather.begin()
+    for copy in own_weights:
+        copy.start()
+    for j in range(1, 8):
+        for copy in weight_copies(j):
+            copy.start()
+
     def arrive(i):
         query_copy(i).wait_recv()
         member = (mine + 4 - i) % 4
         unpack(qraw.at[i - 1], member)
         return member
 
+    for j in range(1, 4):
+        gathers[j].finish()
+        assemble(pieces[j])
+    step(mine, 0, True)
+    conv_gather.relay()
     step(arrive(1), 0, True)
-    gathers[2].relay()
-    begin(3)
+    conv_gather.relay_far()
     step(arrive(3), 0, True)
-    gathers[2].relay_far()
-    gathers[3].relay()
-    conv_gather.begin()
-    for copy in own_weights:
-        copy.start()
     step(arrive(2), 0, True)
-    gathers[3].relay_far()
-    conv_gather.relay()
-    for j in range(1, 8):
-        for copy in weight_copies(j):
-            copy.start()
     finalize(0)
-    gathers[1].finish()
-    assemble(1)
     step(1, 1, True)
-    conv_gather.relay_far()
     finalize(1)
     step(2, 1, False)
-    step(3, 1, False)
-    gathers[2].finish()
-    assemble(2)
     step(2, 2, True)
     finalize(2)
+    step(3, 1, False)
     step(3, 2, False)
-    gathers[3].finish()
-    assemble(3)
     step(3, 3, True)
     finalize(3)
 
@@ -513,13 +553,16 @@
     tokens_gather.drain()
     halo_copy.wait_send()
     for i in range(1, 8):
-        key_copy(i).wait_send()
+        part_copy(i).wait_send()
         moment_copy(i).wait_send()
         for copy in weight_copies(i):
             copy.wait_send()
-    for p in range(4):
-        forward(p).wait_send()
-        gathers[p].drain()
+    for j in range(4):
+        if j > 0:
+            key_copy(j).wait_send()
+        for n in range(3):
+            quad_copy(j, n).wait_send()
+        gathers[j].drain()
     for i in range(1, 4):
         query_copy(i).wait_send()
         member = (mine + i) % 4
@@ -541,15 +584,16 @@
         scratch_shapes=[
             pltpu.VMEM((8, ROWS, 256), bf),
             pltpu.VMEM((ROWS, D_MODEL), bf),
-            pltpu.VMEM((D_MODEL, 512), bf),
-            pltpu.VMEM((D_MODEL, 64), bf),
-            pltpu.VMEM((D_MODEL, 32), bf),
-            pltpu.VMEM((D_MODEL, 256), bf),
+            pltpu.VMEM((D_MODEL, 384), bf),
+            pltpu.VMEM((64, D_MODEL), bf),
+            pltpu.VMEM((128, 256), bf),
+            pltpu.VMEM((256, 256), bf),
             pltpu.VMEM((256, 128), bf),
             pltpu.VMEM((256, 128), bf),
             pltpu.VMEM((ROWS, 128), f32),
             pltpu.VMEM((ROWS, 128), f32),
-            pltpu.VMEM((ROWS, 128), f32),
+            pltpu.VMEM((ROWS, 384), bf),
+            pltpu.VMEM((8, 48, 384), bf),
             pltpu.VMEM((ROWS + ROWS // 2, 128), bf),
             pltpu.VMEM((SHARE, 128), bf),
             pltpu.VMEM((ROWS, 128), bf),
@@ -578,10 +622,10 @@
             pltpu.VMEM((8, 128), f32),
             pltpu.VMEM((8, 8, 128), f32),
             pltpu.VMEM((ROWS, 256), f32),
-            dma((3,)), dma((3,)), dma((8,)), dma((4,)), dma((4,)), dma((4,)), dma((4, 9)), dma((4, 9)),
+            dma((3,)), dma((3,)), dma((4,)), dma((4,)), dma((4, 3)), dma((4, 3)), dma((4, 9)), dma((4, 9)),
             dma((4,)), dma((4,)), dma((4,)), dma((4,)), dma, dma, dma((8,)), dma((8,)),
             dma((9,)), dma((9,)), dma((9,)), dma((9,)), dma((2, 8)), dma((2, 8)), dma((8,)), dma((8,)),
-            dma((2,)), dma((9,)), dma((9,)), dma((11,)),
+            dma((3,)), dma((9,)), dma((9,)), dma((11,)), dma((8,)), dma((8,)),
         ],
         compiler_params=pltpu.CompilerParams(collective_id=1, has_side_effects=True),
         name="layer",
@@ -620,9 +664,9 @@
     return layer(
         tokens,
         query_weight,
-        query_rot_weight,
+        query_rot_weight.T,
         kv_down,
-        rot_down,
+        rot_down.T,
         key_up,
         value_up,
         conv_value_weight,

time: 111 us -> 109 us (0.982)
  the two profiles are of different devices: /device:TPU:467 before, /device:TPU:1 now
where the time goes in v4:
time: 109 us; the launch traced here: 108 us
  Pallas kernels  107 us (98%)
  local copies, waits for them, and re-layouts  1.62 us (1%)
    pallas_call x1, Pallas kernels, layer(): pl.pallas_call(layer_kernel, out_shape=jax.ShapeDtypeStruct((ROWS, 256),...  107 us

profile of v4, /device:TPU:1, one launch (start us, length us, event | category | flops | bytes accessed | tf_op | source)
XLA Modules:
  0.0 108.4 jit_solution(420825407880447919)
XLA Ops:
  0.0 106.7 %layer.1 = bf16[384,256]{1,0:T(8,128)(2,1)} custom-call(bf16[384,256]{1,0:T(8,128)(2,1)} %tokens_hbm.1, bf16[2048,128]{1,0:T(8,128)(2,1)} %query_hbm.1, bf16[64,2048]{1,0:T(8,128)(2,1)} %bitcast.8, bf16[2048,256]{1,0:T(8,128)(2,1)} %kv_down_hbm.1, bf16[32,2048]{1,0:T(8,128)(2,1)} %bitcast.9, bf16[256,128]{1,0:T(8,128)(2,1)} %key_up_hbm.1, ...), custom_call_target="tpu_custom_call" | custom-call | tf_op jit(solution)/shard_map/layer/pallas_call | solution.py:579
  106.7 1.6 %copy.24 = bf16[384,256]{1,0:T(8,128)(2,1)} copy(bf16[384,256]{1,0:T(8,128)(2,1)} %layer.1) | data formatting | bytes 393216

commit v5 on v4

--- a/solution.py
+++ b/solution.py
@@ -100,12 +100,12 @@
     halo, padded, conv_out, mom_send, mom_recv, cbuf, abuf, weights, gains, gain_all, branch,
     q_ssem, q_rsem, k_ssem, k_rsem, f_ssem, f_rsem, ag_ssem, ag_rsem, o_ssem, o_rsem, l_ssem, l_rsem,
     h_ssem, h_rsem, m_ssem, m_rsem, c_ssem, c_rsem, a_ssem, a_rsem, w_ssem, w_rsem, g_ssem, g_rsem,
-    own_sem, t_ssem, t_rsem, load_sem, p_ssem, p_rsem,
+    own_sem, t_ssem, t_rsem, load_sem, p_ssem, p_rsem, v_ssem, v_rsem,
 ):
     sp, tp = lax.axis_index("sp"), lax.axis_index("tp")
     z, y = sp // 8, sp % 8
     kind, mine, parity = (z + z // 2) % 2, z // 2, y % 2
-    residue = (y // 2 + mine) % 4
+    residue = (y // 2 + mine + 2) % 4
     bf, f32 = jnp.bfloat16, jnp.float32
 
     def member_sp(member):
@@ -114,12 +114,10 @@
     place = 2 * parity + z % 2
     z_other, y_other = z + 1 - 2 * (z % 2), y + 1 - 2 * parity
     quad = (z_other * 8 + y, z * 8 + y_other, z_other * 8 + y_other)
-    orders = (0, 1, 3, 2)
-    pieces = [(mine + d) % 4 for d in orders]
-    far_quads = [None]
-    for j in range(1, 4):
-        m = (mine + 4 - orders[j]) % 4
-        far_quads.append((2 * m + z % 2) * 8 + 2 * ((residue + 4 - m) % 4) + parity)
+    key_peers = []
+    for d in range(4):
+        m = (mine + d) % 4
+        key_peers.append((2 * m + z % 2) * 8 + 2 * ((residue + 4 - m) % 4) + parity)
     after, before_sp = (sp + 1) % 64, (sp + 63) % 64
 
     own_rows = pl.ds(pl.multiple_of(256 * tp, 256), 256)
@@ -150,12 +148,14 @@
         pl.semaphore_signal(
             barrier, inc=1, device_id=(member_sp((mine + i) % 4), tp), device_id_type=MESH
         )
-        pl.semaphore_signal(barrier, inc=1, device_id=(far_quads[i], tp), device_id_type=MESH)
         pl.semaphore_signal(barrier, inc=1, device_id=(quad[i - 1], tp), device_id_type=MESH)
+    for peer in key_peers:
+        pl.semaphore_signal(barrier, inc=1, device_id=(peer, tp), device_id_type=MESH)
     for i in range(1, 8):
         pl.semaphore_signal(barrier, inc=1, device_id=(sp, (tp + i) % 8), device_id_type=MESH)
+        pl.semaphore_signal(barrier, inc=1, device_id=(z * 8 + (y + i) % 8, tp), device_id_type=MESH)
     pl.semaphore_signal(barrier, inc=1, device_id=(before_sp, tp), device_id_type=MESH)
-    pl.semaphore_wait(barrier, 17)
+    pl.semaphore_wait(barrier, 25)
 
     def remote(src, dst, ssem, rsem, to):
         return pltpu.make_async_remote_copy(
@@ -170,6 +170,36 @@
 
     tag = lax.broadcasted_iota(jnp.int32, (ROWS, 128), 1)
     low = tag < 64
+    slab = pl.ds(pl.multiple_of(16 * y, 16), 16)
+
+    def weight_copies(j):
+        to = (sp, (tp + j) % 8)
+        columns = pl.ds(pl.multiple_of(256 * ((tp + j) % 8), 256), 256)
+        return (
+            remote(
+                att_w_ref.at[slab, columns], weights.at[0, tp, slab], w_ssem.at[0, j], w_rsem.at[0, tp], to
+            ),
+            remote(
+                conv_w_ref.at[slab, columns], weights.at[1, tp, slab], w_ssem.at[1, j], w_rsem.at[1, tp], to
+            ),
+            remote(gains, gain_all.at[tp], g_ssem.at[j], g_rsem.at[tp], to),
+        )
+
+    own_weights = (
+        pltpu.make_async_copy(att_w_ref.at[slab, own_rows], weights.at[0, tp, slab], own_sem.at[0]),
+        pltpu.make_async_copy(conv_w_ref.at[slab, own_rows], weights.at[1, tp, slab], own_sem.at[1]),
+    )
+
+    def slab_copy(d):
+        rows = weights.at[:, :, slab]
+        return remote(rows, rows, v_ssem.at[d], v_rsem.at[y], (z * 8 + (y + d) % 8, tp))
+
+    gains[...] = jnp.zeros(gains.shape, f32)
+    gains[0:1, :] = att_gain_ref[...]
+    gains[1:2, :] = conv_gain_ref[...]
+    for copy in own_weights:
+        copy.start()
+
     tokens_gather = RingGather(tbuf, 0, ROWS, t_ssem, t_rsem, sp, tp)
     for load in loads[0:3]:
         load.wait()
@@ -197,9 +227,9 @@
         part_copy(j).start()
     tokens_gather.begin()
 
-    gains[...] = jnp.zeros(gains.shape, f32)
-    gains[0:1, :] = att_gain_ref[...]
-    gains[1:2, :] = conv_gain_ref[...]
+    for j in range(1, 8):
+        for copy in weight_copies(j):
+            copy.start()
     for load in loads[3:]:
         load.wait()
     lane = lax.broadcasted_iota(jnp.int32, (256, 128), 1)
@@ -237,54 +267,45 @@
         fold = jnp.where(group == j, pltpu.roll(key_rows[16 * j : 16 * j + 16], 32 * j, 1), fold)
     share_ref[96:112, :] = fold.astype(bf)
 
-    def block(j):
-        return kbuf.at[tp, 4 * pieces[j] + place]
-
-    own_block = pltpu.make_async_copy(share_ref, block(0), own_sem.at[2])
-    own_block.start()
-
-    def key_copy(j):
-        return remote(share_ref, block(0), k_ssem.at[j], k_rsem.at[j], (far_quads[j], tp))
-
-    def quad_copy(j, n):
-        source = share_ref if j == 0 else block(j)
-        return remote(source, block(j), f_ssem.at[j, n], f_rsem.at[j, n], (quad[n], tp))
-
-    def spread(j):
-        if j > 0:
-            remote(share_ref, block(j), k_ssem.at[j], k_rsem.at[j], (far_quads[j], tp)).wait_recv()
+    def block(p):
+        return kbuf.at[tp, 4 * p + place]
+
+    def key_copy(d):
+        return remote(share_ref, block(mine), k_ssem.at[d], k_rsem.at[mine], (key_peers[d], tp))
+
+    def quad_copy(p, n):
+        return remote(block(p), block(p), f_ssem.at[p, n], f_rsem.at[p, n], (quad[n], tp))
+
+    def spread(p):
+        remote(share_ref, block(p), k_ssem.at[0], k_rsem.at[p], (key_peers[0], tp)).wait_recv()
         for n in range(3):
-            quad_copy(j, n).start()
+            quad_copy(p, n).start()
+
+    def begin(p):
+        for n in range(3):
+            quad_copy(p, n).wait_recv()
+        gathers[p].begin()
+
+    for d in range(4):
+        key_copy(d).start()
 
     gathers = [
-        RingGather(kbuf, 4 * p, 4, ag_ssem.at[j], ag_rsem.at[j], sp, tp)
-        for j, p in enumerate(pieces)
+        RingGather(kbuf, 4 * p, 4, ag_ssem.at[p], ag_rsem.at[p], sp, tp) for p in range(4)
     ]
     conv_gather = RingGather(cbuf, 0, ROWS, c_ssem, c_rsem, sp, tp)
     att_gather = RingGather(abuf, 0, ROWS, a_ssem, a_rsem, sp, tp)
 
-    def begin(j):
-        for n in range(3):
-            quad_copy(j, n).wait_recv()
-        gathers[j].begin()
-
-    spread(0)
-    for j in range(1, 4):
-        key_copy(j).start()
-    own_block.wait()
-
     tokens_gather.relay()
     squares = squares + scale_block(tokens_gather.left)
     squares = squares + scale_block(tokens_gather.right)
-    begin(0)
     tokens_gather.relay_far()
-    spread(1)
-    spread(2)
     tokens_gather.finish()
     squares = squares + scale_block(tokens_gather.far)
     for t in (tp, tokens_gather.left, tokens_gather.right, tokens_gather.far):
         squares = squares + scale_block(t + 1 - 2 * (t % 2))
     row_scale = lax.rsqrt(jnp.sum(squares, axis=1, keepdims=True) / D_MODEL + norm_eps)
+    for p in range(4):
+        spread(p)
     flat = lax.dot_general(
         scaled[...], wqr[...], (((1,), (1,)), ((), ())), preferred_element_type=f32
     )
@@ -320,13 +341,9 @@
             rotary = jnp.concatenate([upper, lower], axis=0)
             qbuf[member, h] = jnp.where(low, body, jnp.where(tag < 96, rotary, 0.0)).astype(bf)
 
+    begin(0)
     begin(1)
-    gathers[0].relay()
-    spread(3)
     unpack(q_ref, mine)
-    begin(2)
-    gathers[1].relay()
-    gathers[0].relay_far()
 
     halo_copy.wait_recv()
     edge = halo[...].astype(f32)
@@ -340,9 +357,9 @@
     sum_two = jnp.sum(total * total, axis=1, keepdims=True)
     mom_send[...] = jnp.transpose(jnp.where(tag == 0, sum_one, sum_two))[0:8, :]
 
+    gathers[0].relay()
+    begin(2)
     begin(3)
-    gathers[2].relay()
-    gathers[1].relay_far()
 
     def moment_copy(j):
         return remote(
@@ -442,26 +459,32 @@
             for copy in back_copies(member, mine):
                 copy.start()
 
-    def weight_copies(j):
-        to = (sp, (tp + j) % 8)
-        columns = pl.ds(pl.multiple_of(256 * ((tp + j) % 8), 256), 256)
-        return (
-            remote(att_w_ref.at[:, columns], weights.at[0, tp], w_ssem.at[0, j], w_rsem.at[0, tp], to),
-            remote(conv_w_ref.at[:, columns], weights.at[1, tp], w_ssem.at[1, j], w_rsem.at[1, tp], to),
-            remote(gains, gain_all.at[tp], g_ssem.at[j], g_rsem.at[tp], to),
-        )
-
-    own_columns = pl.ds(pl.multiple_of(256 * tp, 256), 256)
-    own_weights = (
-        pltpu.make_async_copy(att_w_ref.at[:, own_columns], weights.at[0, tp], own_sem.at[0]),
-        pltpu.make_async_copy(conv_w_ref.at[:, own_columns], weights.at[1, tp], own_sem.at[1]),
-    )
-
+    for copy in own_weights:
+        copy.wait()
+    for j in range(1, 8):
+        source = (tp + j) % 8
+        for n in range(2):
+            rows = weights.at[n, source, slab]
+            remote(rows, rows, w_ssem.at[n, j], w_rsem.at[n, source], (sp, source)).wait_recv()
+        remote(gains, gain_all.at[source], g_ssem.at[j], g_rsem.at[source], (sp, source)).wait_recv()
+    for d in range(1, 8):
+        slab_copy(d).start()
+
+    def arrive(i):
+        query_copy(i).wait_recv()
+        member = (mine + 4 - i) % 4
+        unpack(qraw.at[i - 1], member)
+        return member
+
+    gathers[1].relay()
+    gathers[0].relay_far()
+    gathers[0].finish()
+    assemble(0)
+    gathers[2].relay()
+    gathers[1].relay_far()
+    step(mine, 0, True)
     gathers[3].relay()
     gathers[2].relay_far()
-    gathers[0].finish()
-    assemble(pieces[0])
-    gathers[3].relay_far()
 
     mom_recv[tp] = mom_send[...]
     for j in range(1, 8):
@@ -478,49 +501,35 @@
     cbuf[tp] = swished.astype(bf)
 
     conv_gather.begin()
-    for copy in own_weights:
-        copy.start()
-    for j in range(1, 8):
-        for copy in weight_copies(j):
-            copy.start()
-
-    def arrive(i):
-        query_copy(i).wait_recv()
-        member = (mine + 4 - i) % 4
-        unpack(qraw.at[i - 1], member)
-        return member
-
-    for j in range(1, 4):
-        gathers[j].finish()
-        assemble(pieces[j])
-    step(mine, 0, True)
+    step(arrive(1), 0, True)
+    gathers[3].relay_far()
+    step(arrive(3), 0, True)
     conv_gather.relay()
-    step(arrive(1), 0, True)
+    gathers[1].finish()
+    assemble(1)
+    step(arrive(2), 0, True)
     conv_gather.relay_far()
-    step(arrive(3), 0, True)
-    step(arrive(2), 0, True)
     finalize(0)
     step(1, 1, True)
     finalize(1)
     step(2, 1, False)
+    step(3, 1, False)
+    gathers[2].finish()
+    assemble(2)
     step(2, 2, True)
     finalize(2)
-    step(3, 1, False)
     step(3, 2, False)
+    gathers[3].finish()
+    assemble(3)
     step(3, 3, True)
     finalize(3)
 
     gain_all[tp] = gains[...]
     conv_gather.finish()
-    for copy in own_weights:
-        copy.wait()
-    for j in range(1, 8):
-        source = (tp + j) % 8
-        for n in range(2):
-            remote(
-                weights.at[n, source], weights.at[n, source], w_ssem.at[n, j], w_rsem.at[n, source], (sp, source)
-            ).wait_recv()
-        remote(gains, gain_all.at[source], g_ssem.at[j], g_rsem.at[source], (sp, source)).wait_recv()
+    for d in range(1, 8):
+        source = (y + d) % 8
+        rows = weights.at[:, :, pl.ds(pl.multiple_of(16 * source, 16), 16)]
+        remote(rows, rows, v_ssem.at[d], v_rsem.at[source], (z * 8 + source, tp)).wait_recv()
 
     def product(buf, n):
         wide = jnp.concatenate([buf[t] for t in range(8)], axis=1).astype(f32)
@@ -557,9 +566,9 @@
         moment_copy(i).wait_send()
         for copy in weight_copies(i):
             copy.wait_send()
+        slab_copy(i).wait_send()
     for j in range(4):
-        if j > 0:
-            key_copy(j).wait_send()
+        key_copy(j).wait_send()
         for n in range(3):
             quad_copy(j, n).wait_send()
         gathers[j].drain()
@@ -625,7 +634,7 @@
             dma((3,)), dma((3,)), dma((4,)), dma((4,)), dma((4, 3)), dma((4, 3)), dma((4, 9)), dma((4, 9)),
             dma((4,)), dma((4,)), dma((4,)), dma((4,)), dma, dma, dma((8,)), dma((8,)),
             dma((9,)), dma((9,)), dma((9,)), dma((9,)), dma((2, 8)), dma((2, 8)), dma((8,)), dma((8,)),
-            dma((3,)), dma((9,)), dma((9,)), dma((11,)), dma((8,)), dma((8,)),
+            dma((2,)), dma((9,)), dma((9,)), dma((11,)), dma((8,)), dma((8,)), dma((8,)), dma((8,)),
         ],
         compiler_params=pltpu.CompilerParams(collective_id=1, has_side_effects=True),
         name="layer",

time: 109 us -> 93.7 us (0.86)
  Pallas kernels: 107 us -> 90.5 us
    pallas_call x1, Pallas kernels: 107 us -> 90.5 us  [layer(): pl.pallas_call(layer_kernel, out_shape=jax.ShapeDtypeStruct((ROWS, 256),...]
where the time goes in v5:
time: 93.7 us; the launch traced here: 92.2 us
  Pallas kernels  90.5 us (97%)
  local copies, waits for them, and re-layouts  1.62 us (2%)
    pallas_call x1, Pallas kernels, layer(): pl.pallas_call(layer_kernel, out_shape=jax.ShapeDtypeStruct((ROWS, 256),...  90.5 us

profile of v5, /device:TPU:1, one launch (start us, length us, event | category | flops | bytes accessed | tf_op | source)
XLA Modules:
  0.0 92.2 jit_solution(4420679435589699130)
XLA Ops:
  0.0 90.5 %layer.1 = bf16[384,256]{1,0:T(8,128)(2,1)} custom-call(bf16[384,256]{1,0:T(8,128)(2,1)} %tokens_hbm.1, bf16[2048,128]{1,0:T(8,128)(2,1)} %query_hbm.1, bf16[64,2048]{1,0:T(8,128)(2,1)} %bitcast.8, bf16[2048,256]{1,0:T(8,128)(2,1)} %kv_down_hbm.1, bf16[32,2048]{1,0:T(8,128)(2,1)} %bitcast.9, bf16[256,128]{1,0:T(8,128)(2,1)} %key_up_hbm.1, ...), custom_call_target="tpu_custom_call" | custom-call | tf_op jit(solution)/shard_map/layer/pallas_call | solution.py:588
  90.5 1.6 %copy.24 = bf16[384,256]{1,0:T(8,128)(2,1)} copy(bf16[384,256]{1,0:T(8,128)(2,1)} %layer.1) | data formatting | bytes 393216

commit v6 on v5

--- a/solution.py
+++ b/solution.py
@@ -298,14 +298,16 @@
     tokens_gather.relay()
     squares = squares + scale_block(tokens_gather.left)
     squares = squares + scale_block(tokens_gather.right)
+    for p in range(4):
+        spread(p)
     tokens_gather.relay_far()
     tokens_gather.finish()
+    begin(0)
+    begin(1)
     squares = squares + scale_block(tokens_gather.far)
     for t in (tp, tokens_gather.left, tokens_gather.right, tokens_gather.far):
         squares = squares + scale_block(t + 1 - 2 * (t % 2))
     row_scale = lax.rsqrt(jnp.sum(squares, axis=1, keepdims=True) / D_MODEL + norm_eps)
-    for p in range(4):
-        spread(p)
     flat = lax.dot_general(
         scaled[...], wqr[...], (((1,), (1,)), ((), ())), preferred_element_type=f32
     )
@@ -341,9 +343,21 @@
             rotary = jnp.concatenate([upper, lower], axis=0)
             qbuf[member, h] = jnp.where(low, body, jnp.where(tag < 96, rotary, 0.0)).astype(bf)
 
-    begin(0)
-    begin(1)
+    gathers[0].relay()
+    begin(2)
+    for copy in own_weights:
+        copy.wait()
+    for j in range(1, 8):
+        source = (tp + j) % 8
+        for n in range(2):
+            rows = weights.at[n, source, slab]
+            remote(rows, rows, w_ssem.at[n, j], w_rsem.at[n, source], (sp, source)).wait_recv()
+        remote(gains, gain_all.at[source], g_ssem.at[j], g_rsem.at[source], (sp, source)).wait_recv()
+    for d in range(1, 8):
+        slab_copy(d).start()
     unpack(q_ref, mine)
+    gathers[1].relay()
+    begin(3)
 
     halo_copy.wait_recv()
     edge = halo[...].astype(f32)
@@ -356,10 +370,6 @@
     sum_one = jnp.sum(total, axis=1, keepdims=True)
     sum_two = jnp.sum(total * total, axis=1, keepdims=True)
     mom_send[...] = jnp.transpose(jnp.where(tag == 0, sum_one, sum_two))[0:8, :]
-
-    gathers[0].relay()
-    begin(2)
-    begin(3)
 
     def moment_copy(j):
         return remote(
@@ -459,31 +469,19 @@
             for copy in back_copies(member, mine):
                 copy.start()
 
-    for copy in own_weights:
-        copy.wait()
-    for j in range(1, 8):
-        source = (tp + j) % 8
-        for n in range(2):
-            rows = weights.at[n, source, slab]
-            remote(rows, rows, w_ssem.at[n, j], w_rsem.at[n, source], (sp, source)).wait_recv()
-        remote(gains, gain_all.at[source], g_ssem.at[j], g_rsem.at[source], (sp, source)).wait_recv()
-    for d in range(1, 8):
-        slab_copy(d).start()
-
     def arrive(i):
         query_copy(i).wait_recv()
         member = (mine + 4 - i) % 4
         unpack(qraw.at[i - 1], member)
         return member
 
-    gathers[1].relay()
     gathers[0].relay_far()
+    gathers[2].relay()
     gathers[0].finish()
     assemble(0)
-    gathers[2].relay()
     gathers[1].relay_far()
+    gathers[3].relay()
     step(mine, 0, True)
-    gathers[3].relay()
     gathers[2].relay_far()
 
     mom_recv[tp] = mom_send[...]
@@ -500,27 +498,26 @@
     swished = jax.nn.silu(normed * ln_gain_ref[...] + ln_bias_ref[...])
     cbuf[tp] = swished.astype(bf)
 
+    gathers[3].relay_far()
     conv_gather.begin()
     step(arrive(1), 0, True)
-    gathers[3].relay_far()
-    step(arrive(3), 0, True)
-    conv_gather.relay()
     gathers[1].finish()
     assemble(1)
+    step(arrive(3), 0, True)
+    for p in (2, 3):
+        gathers[p].finish()
+        assemble(p)
+    conv_gather.relay()
     step(arrive(2), 0, True)
+    finalize(0)
     conv_gather.relay_far()
-    finalize(0)
     step(1, 1, True)
     finalize(1)
     step(2, 1, False)
-    step(3, 1, False)
-    gathers[2].finish()
-    assemble(2)
     step(2, 2, True)
     finalize(2)
+    step(3, 1, False)
     step(3, 2, False)
-    gathers[3].finish()
-    assemble(3)
     step(3, 3, True)
     finalize(3)
 

time: 93.7 us -> 89.7 us (0.957); the launches traced: 92.2 us -> 89.5 us
  Pallas kernels: 90.5 us -> 87.8 us
    pallas_call x1, Pallas kernels: 90.5 us -> 87.8 us  [layer(): pl.pallas_call(layer_kernel, out_shape=jax.ShapeDtypeStruct((ROWS, 256),...]
where the time goes in v6:
time: 89.7 us; the launch traced here: 89.5 us
  Pallas kernels  87.8 us (98%)
  local copies, waits for them, and re-layouts  1.62 us (2%)
    pallas_call x1, Pallas kernels, layer(): pl.pallas_call(layer_kernel, out_shape=jax.ShapeDtypeStruct((ROWS, 256),...  87.8 us

profile of v6, /device:TPU:1, one launch (start us, length us, event | category | flops | bytes accessed | tf_op | source)
XLA Modules:
  0.0 89.5 jit_solution(7852021665671119457)
XLA Ops:
  0.0 87.8 %layer.1 = bf16[384,256]{1,0:T(8,128)(2,1)} custom-call(bf16[384,256]{1,0:T(8,128)(2,1)} %tokens_hbm.1, bf16[2048,128]{1,0:T(8,128)(2,1)} %query_hbm.1, bf16[64,2048]{1,0:T(8,128)(2,1)} %bitcast.8, bf16[2048,256]{1,0:T(8,128)(2,1)} %kv_down_hbm.1, bf16[32,2048]{1,0:T(8,128)(2,1)} %bitcast.9, bf16[256,128]{1,0:T(8,128)(2,1)} %key_up_hbm.1, ...), custom_call_target="tpu_custom_call" | custom-call | tf_op jit(solution)/shard_map/layer/pallas_call | solution.py:585
  87.8 1.6 %copy.24 = bf16[384,256]{1,0:T(8,128)(2,1)} copy(bf16[384,256]{1,0:T(8,128)(2,1)} %layer.1) | data formatting | bytes 393216

commit v7 on v6

--- a/solution.py
+++ b/solution.py
@@ -120,6 +120,19 @@
         key_peers.append((2 * m + z % 2) * 8 + 2 * ((residue + 4 - m) % 4) + parity)
     after, before_sp = (sp + 1) % 64, (sp + 63) % 64
 
+    barrier = pltpu.get_barrier_semaphore()
+    for i in range(1, 4):
+        pl.semaphore_signal(
+            barrier, inc=1, device_id=(member_sp((mine + i) % 4), tp), device_id_type=MESH
+        )
+        pl.semaphore_signal(barrier, inc=1, device_id=(quad[i - 1], tp), device_id_type=MESH)
+    for peer in key_peers:
+        pl.semaphore_signal(barrier, inc=1, device_id=(peer, tp), device_id_type=MESH)
+    for i in range(1, 8):
+        pl.semaphore_signal(barrier, inc=1, device_id=(sp, (tp + i) % 8), device_id_type=MESH)
+        pl.semaphore_signal(barrier, inc=1, device_id=(z * 8 + (y + i) % 8, tp), device_id_type=MESH)
+    pl.semaphore_signal(barrier, inc=1, device_id=(before_sp, tp), device_id_type=MESH)
+
     own_rows = pl.ds(pl.multiple_of(256 * tp, 256), 256)
     wrd[32:128, :] = jnp.zeros((96, 256), bf)
     loads = [
@@ -143,20 +156,6 @@
     for load in loads:
         load.start()
 
-    barrier = pltpu.get_barrier_semaphore()
-    for i in range(1, 4):
-        pl.semaphore_signal(
-            barrier, inc=1, device_id=(member_sp((mine + i) % 4), tp), device_id_type=MESH
-        )
-        pl.semaphore_signal(barrier, inc=1, device_id=(quad[i - 1], tp), device_id_type=MESH)
-    for peer in key_peers:
-        pl.semaphore_signal(barrier, inc=1, device_id=(peer, tp), device_id_type=MESH)
-    for i in range(1, 8):
-        pl.semaphore_signal(barrier, inc=1, device_id=(sp, (tp + i) % 8), device_id_type=MESH)
-        pl.semaphore_signal(barrier, inc=1, device_id=(z * 8 + (y + i) % 8, tp), device_id_type=MESH)
-    pl.semaphore_signal(barrier, inc=1, device_id=(before_sp, tp), device_id_type=MESH)
-    pl.semaphore_wait(barrier, 25)
-
     def remote(src, dst, ssem, rsem, to):
         return pltpu.make_async_remote_copy(
             src_ref=src, dst_ref=dst, send_sem=ssem, recv_sem=rsem, device_id=to, device_id_type=MESH
@@ -223,6 +222,7 @@
             (sp, peer),
         )
 
+    pl.semaphore_wait(barrier, 25)
     for j in range(1, 8):
         part_copy(j).start()
     tokens_gather.begin()
@@ -484,6 +484,14 @@
     step(mine, 0, True)
     gathers[2].relay_far()
 
+    gathers[3].relay_far()
+    step(arrive(1), 0, True)
+    gathers[1].finish()
+    assemble(1)
+    step(arrive(3), 0, True)
+    for p in (2, 3):
+        gathers[p].finish()
+        assemble(p)
     mom_recv[tp] = mom_send[...]
     for j in range(1, 8):
         source = (tp + j) % 8
@@ -498,24 +506,16 @@
     swished = jax.nn.silu(normed * ln_gain_ref[...] + ln_bias_ref[...])
     cbuf[tp] = swished.astype(bf)
 
-    gathers[3].relay_far()
     conv_gather.begin()
-    step(arrive(1), 0, True)
-    gathers[1].finish()
-    assemble(1)
-    step(arrive(3), 0, True)
-    for p in (2, 3):
-        gathers[p].finish()
-        assemble(p)
-    conv_gather.relay()
     step(arrive(2), 0, True)
     finalize(0)
-    conv_gather.relay_far()
     step(1, 1, True)
     finalize(1)
     step(2, 1, False)
+    conv_gather.relay()
     step(2, 2, True)
     finalize(2)
+    conv_gather.relay_far()
     step(3, 1, False)
     step(3, 2, False)
     step(3, 3, True)

time: 89.7 us -> 90.2 us (level)
  no operation moved by 1% of the time
where the time goes in v7:
time: 90.2 us; the launch traced here: 90 us
  Pallas kernels  88.4 us (98%)
  local copies, waits for them, and re-layouts  1.62 us (2%)
    pallas_call x1, Pallas kernels, layer(): pl.pallas_call(layer_kernel, out_shape=jax.ShapeDtypeStruct((ROWS, 256),...  88.4 us

profile of v7, /device:TPU:1, one launch (start us, length us, event | category | flops | bytes accessed | tf_op | source)
XLA Modules:
  0.0 90.0 jit_solution(7982949155566614334)
XLA Ops:
  0.0 88.4 %layer.1 = bf16[384,256]{1,0:T(8,128)(2,1)} custom-call(bf16[384,256]{1,0:T(8,128)(2,1)} %tokens_hbm.1, bf16[2048,128]{1,0:T(8,128)(2,1)} %query_hbm.1, bf16[64,2048]{1,0:T(8,128)(2,1)} %bitcast.8, bf16[2048,256]{1,0:T(8,128)(2,1)} %kv_down_hbm.1, bf16[32,2048]{1,0:T(8,128)(2,1)} %bitcast.9, bf16[256,128]{1,0:T(8,128)(2,1)} %key_up_hbm.1, ...), custom_call_target="tpu_custom_call" | custom-call | tf_op jit(solution)/shard_map/layer/pallas_call | solution.py:585
  88.4 1.6 %copy.24 = bf16[384,256]{1,0:T(8,128)(2,1)} copy(bf16[384,256]{1,0:T(8,128)(2,1)} %layer.1) | data formatting | bytes 393216

commit v8 on v6

--- a/solution.py
+++ b/solution.py
@@ -293,7 +293,9 @@
         RingGather(kbuf, 4 * p, 4, ag_ssem.at[p], ag_rsem.at[p], sp, tp) for p in range(4)
     ]
     conv_gather = RingGather(cbuf, 0, ROWS, c_ssem, c_rsem, sp, tp)
-    att_gather = RingGather(abuf, 0, ROWS, a_ssem, a_rsem, sp, tp)
+    att_gathers = [
+        RingGather(abuf, 192 * n, 192, a_ssem.at[n], a_rsem.at[n], sp, tp) for n in range(2)
+    ]
 
     tokens_gather.relay()
     squares = squares + scale_block(tokens_gather.left)
@@ -442,10 +444,19 @@
 
     def back_copies(member, source):
         to = (member_sp(member), tp)
-        return (
-            remote(o_send.at[member], o_recv.at[source], o_ssem.at[member], o_rsem.at[source], to),
-            remote(l_send.at[member], l_recv.at[source], l_ssem.at[member], l_rsem.at[source], to),
-        )
+        copies = [remote(l_send.at[member], l_recv.at[source], l_ssem.at[member], l_rsem.at[source], to)]
+        for n in range(2):
+            rows = pl.ds(192 * n, 192)
+            copies.append(
+                remote(
+                    o_send.at[member, rows],
+                    o_recv.at[source, rows],
+                    o_ssem.at[n, member],
+                    o_rsem.at[n, source],
+                    to,
+                )
+            )
+        return copies
 
     def finalize(member):
         sums, tops = [], []
@@ -537,24 +548,32 @@
 
     branch[...] = product(cbuf, 1)
 
-    logs, values = [own_lse[...]], [own_out[...]]
+    logs = [own_lse[...]]
     for i in range(1, 4):
         source = (mine + i) % 4
-        for copy in back_copies(source, source):
-            copy.wait_recv()
+        back_copies(source, source)[0].wait_recv()
         columns = jnp.transpose(l_recv[source])
         logs.append(jnp.where(low, columns[:, 0:1], columns[:, 4:5]))
-        values.append(o_recv[source].astype(f32))
     peak = jnp.maximum(jnp.maximum(logs[0], logs[1]), jnp.maximum(logs[2], logs[3]))
     shares = [jnp.exp2(log - peak) for log in logs]
-    merged = sum(s * v for s, v in zip(shares, values)) / sum(shares)
-    abuf[tp] = merged.astype(bf)
-
-    att_gather.begin()
-    att_gather.relay()
-    att_gather.relay_far()
-    att_gather.finish()
-    out_ref[...] = (branch[...] + product(abuf, 0)).astype(bf)
+    whole = sum(shares)
+    for n in range(2):
+        rows = slice(192 * n, 192 * n + 192)
+        merged = shares[0][rows] * own_out[rows, :]
+        for i in range(1, 4):
+            source = (mine + i) % 4
+            back_copies(source, source)[1 + n].wait_recv()
+            merged = merged + shares[i][rows] * o_recv[source, rows, :].astype(f32)
+        abuf[tp, rows, :] = (merged / whole[rows]).astype(bf)
+        att_gathers[n].begin()
+
+    for gather in att_gathers:
+        gather.relay()
+    for gather in att_gathers:
+        gather.relay_far()
+    for gather in att_gathers:
+        gather.finish()
+    out_ref[...] = branch[...] + product(abuf, 0)
 
     tokens_gather.drain()
     halo_copy.wait_send()
@@ -575,7 +594,8 @@
         for copy in back_copies(member, mine):
             copy.wait_send()
     conv_gather.drain()
-    att_gather.drain()
+    for gather in att_gathers:
+        gather.drain()
 
 
 def layer(*args):
@@ -584,7 +604,7 @@
     dma = pltpu.SemaphoreType.DMA
     return pl.pallas_call(
         layer_kernel,
-        out_shape=jax.ShapeDtypeStruct((ROWS, 256), bf),
+        out_shape=jax.ShapeDtypeStruct((ROWS, 256), f32),
         in_specs=[anywhere] * 13 + [vmem] * 9,
         out_specs=vmem,
         scratch_shapes=[
@@ -629,8 +649,8 @@
             pltpu.VMEM((8, 8, 128), f32),
             pltpu.VMEM((ROWS, 256), f32),
             dma((3,)), dma((3,)), dma((4,)), dma((4,)), dma((4, 3)), dma((4, 3)), dma((4, 9)), dma((4, 9)),
-            dma((4,)), dma((4,)), dma((4,)), dma((4,)), dma, dma, dma((8,)), dma((8,)),
-            dma((9,)), dma((9,)), dma((9,)), dma((9,)), dma((2, 8)), dma((2, 8)), dma((8,)), dma((8,)),
+            dma((2, 4)), dma((2, 4)), dma((4,)), dma((4,)), dma, dma, dma((8,)), dma((8,)),
+            dma((9,)), dma((9,)), dma((2, 9)), dma((2, 9)), dma((2, 8)), dma((2, 8)), dma((8,)), dma((8,)),
             dma((2,)), dma((9,)), dma((9,)), dma((11,)), dma((8,)), dma((8,)), dma((8,)), dma((8,)),
         ],
         compiler_params=pltpu.CompilerParams(collective_id=1, has_side_effects=True),
@@ -690,7 +710,7 @@
         conv_ln_bias[None, :],
         att_out_gain[None, :],
         conv_out_gain[None, :],
-    )
+    ).astype(jnp.bfloat16)
 
 
 def solution(mesh):

time: 89.7 us -> 90.4 us (level)
  other arithmetic: 0 us -> 1.69 us
  local copies, waits for them, and re-layouts: 1.62 us -> 0 us
    convert_element_type x0 -> x1, other arithmetic: none -> 1.69 us  [shards(): return layer(tokens, query_weight, query_rot_weight.T, kv_down, rot_down....]
    unnamed x1 -> x0, local copies, waits for them, and re-layouts: 1.62 us -> none
where the time goes in v8:
time: 90.4 us; the launch traced here: 90.2 us
  Pallas kernels  88.5 us (98%)
  other arithmetic  1.69 us (2%)
    pallas_call x1, Pallas kernels, layer(): pl.pallas_call(layer_kernel, out_shape=jax.ShapeDtypeStruct((ROWS, 256),...  88.5 us

profile of v8, /device:TPU:1, one launch (start us, length us, event | category | flops | bytes accessed | tf_op | source)
XLA Modules:
  0.0 90.2 jit_solution(16263462376847107831)
XLA Ops:
  0.0 88.5 %layer.1 = f32[384,256]{1,0:T(8,128)} custom-call(bf16[384,256]{1,0:T(8,128)(2,1)} %tokens_hbm.1, bf16[2048,128]{1,0:T(8,128)(2,1)} %query_hbm.1, bf16[64,2048]{1,0:T(8,128)(2,1)} %bitcast.8, bf16[2048,256]{1,0:T(8,128)(2,1)} %kv_down_hbm.1, bf16[32,2048]{1,0:T(8,128)(2,1)} %bitcast.9, bf16[256,128]{1,0:T(8,128)(2,1)} %key_up_hbm.1, ...), custom_call_target="tpu_custom_call" | custom-call | tf_op jit(solution)/shard_map/layer/pallas_call | solution.py:605
  88.5 1.7 %convert_element_type.3 = bf16[384,256]{1,0:T(8,128)(2,1)} convert(f32[384,256]{1,0:T(8,128)} %layer.1) | non-fusion elementwise | flops 98304 | bytes 589824 | tf_op jit(solution)/shard_map/convert_element_type | solution.py:713

commit v9 on v6

--- a/solution.py
+++ b/solution.py
@@ -480,9 +480,14 @@
     gathers[0].finish()
     assemble(0)
     gathers[1].relay_far()
+    step(mine, 0, True)
     gathers[3].relay()
-    step(mine, 0, True)
+    gathers[1].finish()
+    assemble(1)
     gathers[2].relay_far()
+    step(arrive(1), 0, True)
+    gathers[3].relay_far()
+    step(arrive(3), 0, True)
 
     mom_recv[tp] = mom_send[...]
     for j in range(1, 8):
@@ -498,26 +503,22 @@
     swished = jax.nn.silu(normed * ln_gain_ref[...] + ln_bias_ref[...])
     cbuf[tp] = swished.astype(bf)
 
-    gathers[3].relay_far()
     conv_gather.begin()
-    step(arrive(1), 0, True)
-    gathers[1].finish()
-    assemble(1)
-    step(arrive(3), 0, True)
-    for p in (2, 3):
-        gathers[p].finish()
-        assemble(p)
-    conv_gather.relay()
+    gathers[2].finish()
+    assemble(2)
     step(arrive(2), 0, True)
     finalize(0)
-    conv_gather.relay_far()
     step(1, 1, True)
     finalize(1)
     step(2, 1, False)
+    conv_gather.relay()
     step(2, 2, True)
     finalize(2)
     step(3, 1, False)
+    conv_gather.relay_far()
     step(3, 2, False)
+    gathers[3].finish()
+    assemble(3)
     step(3, 3, True)
     finalize(3)
 

time: 89.7 us -> 88.4 us (0.986)
  the two profiles are of different devices: /device:TPU:1 before, /device:TPU:451 now
where the time goes in v9:
time: 88.4 us; the launch traced here: 88.2 us
  Pallas kernels  86.6 us (98%)
  local copies, waits for them, and re-layouts  1.62 us (2%)
    pallas_call x1, Pallas kernels, layer(): pl.pallas_call(layer_kernel, out_shape=jax.ShapeDtypeStruct((ROWS, 256),...  86.6 us

profile of v9, /device:TPU:451, one launch (start us, length us, event | category | flops | bytes accessed | tf_op | source)
XLA Modules:
  0.0 88.2 jit_solution(13715806414670926580)
XLA Ops:
  0.0 86.6 %layer.1 = bf16[384,256]{1,0:T(8,128)(2,1)} custom-call(bf16[384,256]{1,0:T(8,128)(2,1)} %tokens_hbm.1, bf16[2048,128]{1,0:T(8,128)(2,1)} %query_hbm.1, bf16[64,2048]{1,0:T(8,128)(2,1)} %bitcast.8, bf16[2048,256]{1,0:T(8,128)(2,1)} %kv_down_hbm.1, bf16[32,2048]{1,0:T(8,128)(2,1)} %bitcast.9, bf16[256,128]{1,0:T(8,128)(2,1)} %key_up_hbm.1, ...), custom_call_target="tpu_custom_call" | custom-call | tf_op jit(solution)/shard_map/layer/pallas_call | solution.py:586
  86.6 1.6 %copy.24 = bf16[384,256]{1,0:T(8,128)(2,1)} copy(bf16[384,256]{1,0:T(8,128)(2,1)} %layer.1) | data formatting | bytes 393216
